TPU v7x, 128 devices: a whole 4x4x4 slice. The times are simulated.
128 devices in a mesh: sp: 16 (over z, y), dp: 8 (over x, core).
Axes of the slice: x: 4, y: 4, z: 4, core: 2. Of those that a mesh axis runs over, the one named last changes fastest.
Arguments:
- hidden_in: bfloat16 [8, 2048, 2048], P('dp', 'sp'), may hold values from -6 to 6
- queries: bfloat16 [8, 2048, 1536], P('dp', 'sp'), may hold values from -64 to 64
- key_value_latent: bfloat16 [8, 2048, 512], P('dp', 'sp'), may hold values from -6 to 6
- keys_rope: bfloat16 [8, 2048, 32], P('dp', 'sp'), may hold values from -4 to 4
- latent_norm_gain: float32 [512], replicated, may hold values from 0.1 to 1.9
- latent_up_weight: bfloat16 [512, 2048], replicated, may hold values from -0.25 to 0.25
- attn_gain: float32 [1024], replicated, may hold values from 0.1 to 1.9
- out_proj: bfloat16 [1024, 2048], replicated, may hold values from -0.1875 to 0.1875
- norm1_gain: float32 [2048], replicated, may hold values from 0.1 to 1.9
- norm1_bias: float32 [2048], replicated, may hold values from -1.5 to 1.5
- expert_ids: int32 [8, 2048, 4], P('dp', 'sp'), may hold values from 0 to 127, all different within a row; in each aligned block of 128 rows (0 to 127, 128 to 255, ..., all dimensions but the last counted through in order) at most 6 rows name the same one
- route_weights: float32 [8, 2048, 4], P('dp', 'sp'), may hold values from 0.1 to 1
- gate_proj: bfloat16 [128, 2048, 512], P(('sp', 'dp')), may hold values from -0.125 to 0.125
- up_proj: bfloat16 [128, 2048, 512], P(('sp', 'dp')), may hold values from -0.125 to 0.125
- down_proj: bfloat16 [128, 512, 2048], P(('sp', 'dp')), may hold values from -0.25 to 0.25
- shared_gate: bfloat16 [2048, 512], replicated, may hold values from -0.125 to 0.125
- shared_up: bfloat16 [2048, 512], replicated, may hold values from -0.125 to 0.125
- shared_down: bfloat16 [512, 2048], replicated, may hold values from -0.25 to 0.25
- norm2_gain: float32 [2048], replicated, may hold values from 0.1 to 1.9
- norm2_bias: float32 [2048], replicated, may hold values from -1.5 to 1.5
Outputs:
- result: bfloat16 [8, 2048, 2048], P('dp', 'sp')
Inputs may be any that keep to these rules, and one draw needn't show every extreme that they name: `expert_ids`: each row names 4 different experts. Among the rows of one device (aligned blocks of 128 rows), no expert is named more than 6 times, a bound that some block reaches.
All inputs are finite; a program needn't handle non-finite values.
Results may differ from a plain program's by a relative error of at most 0.01.
Values may be sent and summed in bfloat16 or wider, within the bound.
A program may use at most 128 MiB of HBM per device.

v0:
```python
import math

import jax
import jax.numpy as jnp
from jax import lax
from jax.sharding import PartitionSpec as P

D = 2048
ATTENTION_HEADS = 16
PLAIN_HEAD_WIDTH = 64
QK_ROPE = 32
VALUE_HEAD_WIDTH = 64
TOP_K = 4


ALPHA = 2.0**0.25
ROUTED = 2.5
THETA = 10000.0


def copy_for_each(value, axis):
    size = lax.axis_size(axis)
    return lax.all_to_all(
        jnp.broadcast_to(value[None], (size, *value.shape)), axis, 0, 0, tiled=True
    )


def in_order(tiles, dim):
    lengths = list(tiles.shape[1:])
    lengths[dim] *= tiles.shape[0]
    return jnp.moveaxis(tiles, 0, dim).reshape(lengths)


def collect(value, axis, dim):
    tiles = copy_for_each(value, axis)
    return in_order(tiles, dim)


def rms_scaled(values, scaling):
    widened = values.astype(jnp.float32)
    return (
        widened * lax.rsqrt(jnp.mean(widened * widened, axis=-1, keepdims=True) + 1e-06) * scaling
    )


def layer_norm(values, scaling, bias_add):
    centre = values - jnp.mean(values, axis=-1, keepdims=True)
    spread = jnp.mean(centre * centre, axis=-1, keepdims=True)
    return centre * lax.rsqrt(spread + 1e-05) * scaling + bias_add


def rotation_tables(positions, rot_width):
    frequency = THETA ** (-jnp.arange(0, rot_width, 2, dtype=jnp.float32) / rot_width)
    angles = positions.astype(jnp.float32)[:, None] * frequency[None, :]
    return (jnp.cos(angles), jnp.sin(angles))


def turn(values, cosine_table, sine_table):
    half_width = values.shape[-1] // 2
    first_half = values[..., :half_width]
    second_half = values[..., half_width:]
    return jnp.concatenate(
        [
            first_half * cosine_table - second_half * sine_table,
            second_half * cosine_table + first_half * sine_table,
        ],
        axis=-1,
    )


def attend(query, key_full, values):
    length = query.shape[0]
    span_rows = 512
    block_count = length // span_rows
    blocks = query.reshape(block_count, span_rows, query.shape[1])
    key_pos = jnp.arange(length, dtype=jnp.int32)
    factor = 1.0 / math.sqrt(query.shape[1])

    def one_block(inputs):
        block_index, query_rows = inputs
        scores = jnp.dot(query_rows, key_full.T, preferred_element_type=jnp.float32) * factor
        query_pos = block_index * span_rows + jnp.arange(span_rows, dtype=jnp.int32)
        scores = jnp.where(key_pos[None, :] <= query_pos[:, None], scores, -jnp.inf)
        row_max = jnp.max(scores, axis=-1, keepdims=True)
        weights = jnp.exp(scores - row_max)
        weights = (weights / jnp.sum(weights, axis=-1, keepdims=True)).astype(jnp.bfloat16)
        return jnp.dot(weights, values, preferred_element_type=jnp.float32).astype(jnp.bfloat16)

    attended = lax.map(one_block, (jnp.arange(block_count, dtype=jnp.int32), blocks))
    return attended.reshape(length, values.shape[1])


def swiglu_rows(rows, gate_mat, up_mat, down_mat):
    gated = jnp.dot(rows, gate_mat, preferred_element_type=jnp.float32)
    lifted = jnp.dot(rows, up_mat, preferred_element_type=jnp.float32)
    inner = (jax.nn.silu(gated) * lifted).astype(jnp.bfloat16)
    return jnp.dot(inner, down_mat, preferred_element_type=jnp.float32)


def per_device(
    hidden_in,
    queries,
    key_value_latent,
    keys_rope,
    latent_norm_gain,
    latent_up_weight,
    attn_gain,
    out_proj,
    norm1_gain,
    norm1_bias,
    expert_ids,
    route_weights,
    gate_proj,
    up_proj,
    down_proj,
    shared_gate,
    shared_up,
    shared_down,
    norm2_gain,
    norm2_bias,
):
    seq_devices = lax.axis_size("sp")
    tok_rows = hidden_in.shape[1]
    length = tok_rows * seq_devices
    heads_here = ATTENTION_HEADS // seq_devices
    normed = rms_scaled(key_value_latent[0], latent_norm_gain).astype(jnp.bfloat16)
    keys_values = jnp.dot(normed, latent_up_weight, preferred_element_type=jnp.float32).astype(
        jnp.bfloat16
    )
    local_pos = lax.axis_index("sp") * tok_rows + jnp.arange(tok_rows, dtype=jnp.int32)
    cos_local, sin_local = rotation_tables(local_pos, QK_ROPE)
    keys_turned = turn(keys_rope[0].astype(jnp.float32), cos_local, sin_local).astype(jnp.bfloat16)
    query_send = queries[0].reshape(
        tok_rows, seq_devices, heads_here * (PLAIN_HEAD_WIDTH + QK_ROPE)
    )
    pair_send = keys_values.reshape(
        tok_rows, seq_devices, heads_here * (PLAIN_HEAD_WIDTH + VALUE_HEAD_WIDTH)
    )
    query_heads, pair_heads = (
        lax.all_to_all(query_send, "sp", split_axis=1, concat_axis=0, tiled=True),
        lax.all_to_all(pair_send, "sp", split_axis=1, concat_axis=0, tiled=True),
    )
    keys_whole = collect(keys_turned, "sp", 0)
    cos_whole, sin_whole = rotation_tables(jnp.arange(length, dtype=jnp.int32), QK_ROPE)
    query_turned = turn(
        query_heads[..., PLAIN_HEAD_WIDTH:].astype(jnp.float32),
        cos_whole[:, None, :],
        sin_whole[:, None, :],
    ).astype(jnp.bfloat16)
    query_full = jnp.concatenate([query_heads[..., :PLAIN_HEAD_WIDTH], query_turned], axis=-1)
    key_full = jnp.concatenate(
        [pair_heads[..., :PLAIN_HEAD_WIDTH], keys_whole[:, None, :]], axis=-1
    )
    values_heads = pair_heads[..., PLAIN_HEAD_WIDTH:]
    by_head = lax.map(
        lambda inputs: attend(inputs[0], inputs[1], inputs[2]),
        (
            jnp.moveaxis(query_full, 1, 0),
            jnp.moveaxis(key_full, 1, 0),
            jnp.moveaxis(values_heads, 1, 0),
        ),
    )
    outgoing = jnp.moveaxis(by_head, 0, 1).reshape(
        seq_devices, tok_rows, heads_here * VALUE_HEAD_WIDTH
    )
    incoming = lax.all_to_all(outgoing, "sp", split_axis=0, concat_axis=2, tiled=True)
    attn_normed = rms_scaled(incoming[0], attn_gain).astype(jnp.bfloat16)
    mixed = jnp.dot(attn_normed, out_proj, preferred_element_type=jnp.float32)
    first = layer_norm(
        ALPHA * hidden_in[0].astype(jnp.float32) + mixed, norm1_gain, norm1_bias
    ).astype(jnp.bfloat16)
    group = lax.axis_size("sp") * lax.axis_size("dp")
    capacity = (tok_rows * TOP_K * 3 + 2 * group - 1) // (2 * group)
    entries = expert_ids[0].reshape(-1)
    onehot = (entries[:, None] == jnp.arange(group, dtype=jnp.int32)[None, :]).astype(jnp.int32)
    earlier = jnp.cumsum(onehot, axis=0) - onehot
    slots = jnp.sum(earlier * onehot, axis=-1)
    places = (entries * capacity + slots).reshape(tok_rows, TOP_K)
    slot_ids = jnp.arange(group * capacity, dtype=jnp.int32)
    dispatch = jnp.any(places[None, :, :] == slot_ids[:, None, None], axis=-1).astype(jnp.bfloat16)
    outbound = jnp.dot(dispatch, first, preferred_element_type=jnp.float32).astype(jnp.bfloat16)
    arrived = lax.all_to_all(
        outbound.reshape(group, capacity, D), ("sp", "dp"), split_axis=0, concat_axis=0, tiled=True
    )
    flat_rows = arrived.reshape(group * capacity, D)
    produced = (
        swiglu_rows(flat_rows, gate_proj[0], up_proj[0], down_proj[0])
        .astype(jnp.bfloat16)
        .reshape(group, capacity, D)
    )
    returned = lax.all_to_all(produced, ("sp", "dp"), split_axis=0, concat_axis=0, tiled=True)
    returned_flat = returned.reshape(group * capacity, D)
    weights = route_weights[0]
    gates = weights / jnp.sum(weights, axis=-1, keepdims=True) * ROUTED
    routed = jnp.zeros((tok_rows, D), jnp.float32)
    for column in range(TOP_K):
        picker = (places[:, column : column + 1] == slot_ids[None, :]).astype(jnp.bfloat16)
        picked = jnp.dot(picker, returned_flat, preferred_element_type=jnp.float32)
        routed = routed + gates[:, column : column + 1] * picked
    feed = routed + swiglu_rows(first, shared_gate, shared_up, shared_down)
    result = layer_norm(ALPHA * first.astype(jnp.float32) + feed, norm2_gain, norm2_bias).astype(
        jnp.bfloat16
    )
    return result.reshape(1, tok_rows, D)


def solution(mesh):
    in_specs = (
        P("dp", "sp", None),
        P("dp", "sp", None),
        P("dp", "sp", None),
        P("dp", "sp", None),
        P(),
        P(),
        P(),
        P(),
        P(),
        P(),
        P("dp", "sp", None),
        P("dp", "sp", None),
        P(("sp", "dp"), None, None),
        P(("sp", "dp"), None, None),
        P(("sp", "dp"), None, None),
        P(),
        P(),
        P(),
        P(),
        P(),
    )
    out_specs = P("dp", "sp", None)
    return jax.shard_map(
        per_device, mesh=mesh, in_specs=in_specs, out_specs=out_specs, check_vma=False
    )
```

profile of v0, /device:TPU:1, one launch (start us, length us, event | category | flops | bytes accessed | tf_op | source)
XLA Modules:
  0.0 257.5 jit_solution(6915109282464241579)
XLA Ops:
  1.7 8.6 %all-to-all-start.2 = ((bf16[16,128,32]{1,2,0:T(8,128)(2,1)}), bf16[16,128,32]{1,2,0:T(8,128)(2,1)S(1)}, u32[]{:S(2)}, u32[]{:S(2)}) async-start(bf16[16,128,32]{1,2,0:T(8,128)(2,1)} %broadcast_in_dim.10), calls=%async_computation.2 | async-start | bytes 262144 | tf_op jit(solution)/shard_map/all_to_all | solution.py:23
  11.3 1.9 copy.77
  14.2 2.2 fusion.23
  17.7 6.7 %all-to-all-start = ((bf16[128,16,96]{0,2,1:T(8,128)(2,1)}), bf16[128,16,96]{0,2,1:T(8,128)(2,1)S(1)}, u32[]{:S(2)}, u32[]{:S(2)}) async-start(bf16[128,16,96]{0,2,1:T(8,128)(2,1)} %bitcast.1), calls=%async_computation | async-start | bytes 786432 | tf_op jit(solution)/shard_map/all_to_all | solution.py:140
  25.7 7.3 %all-to-all-done = bf16[128,16,96]{0,2,1:T(8,128)(2,1)S(1)} async-done(((bf16[128,16,96]{0,2,1:T(8,128)(2,1)}), bf16[128,16,96]{0,2,1:T(8,128)(2,1)S(1)}, u32[]{:S(2)}, u32[]{:S(2)}) %all-to-all-start) | async-done | bytes 393248 | tf_op jit(solution)/shard_map/all_to_all | solution.py:140
  33.8 3.6 %all-to-all-start.1 = ((bf16[128,16,128]{2,0,1:T(8,128)(2,1)}), bf16[128,16,128]{2,0,1:T(8,128)(2,1)S(1)}, u32[]{:S(2)}, u32[]{:S(2)}) async-start(bf16[128,16,128]{2,0,1:T(8,128)(2,1)} %bitcast.135), calls=%async_computation.1 | async-start | bytes 1048576 | tf_op jit(solution)/shard_map/all_to_all | solution.py:141
  38.5 1.2 fusion.52
  39.7 1.9 copy.94
  43.6 2.7 %pad_maximum_fusion = bf16[4,512,96]{2,1,0:T(8,128)(2,1)} fusion(bf16[4,512,16]{2,1,0:T(8,128)(2,1)} %bitcast.137, bf16[4,512,16]{2,1,0:T(8,128)(2,1)} %bitcast.136, bf16[4,512,64]{2,1,0:T(8,128)(2,1)} %bitcast.138), kind=kLoop, calls=%fused_computation.46 | loop fusion | flops 1179648 | bytes 786432 | tf_op jit(solution)/shard_map/concatenate | solution.py:150
  48.0 21.5 %while.18 = (s32[]{:T(128)}, bf16[4,512,64]{1,2,0:T(8,128)(2,1)S(1)}, s32[4]{0:T(128)S(1)}, bf16[4,512,96]{2,1,0:T(8,128)(2,1)}, bf16[2048,96]{1,0:T(8,128)(2,1)...) while((s32[]{:T(128)}, bf16[4,512,64]{1,2,0:T(8,128)(2,1)S(1)}, s32[4]{0:T(128)S(1)}, ...), condition=%wide.region_4.5_spmd.clone, body=%wide.region_1.4_spmd.clone.sunk | while | flops 345013760 | bytes 14760593 | solution.py:89
  49.4 1.9 fusion.102
  52.3 1.1 fusion.104
  54.8 1.9 fusion.102
  60.2 1.9 fusion.102
  65.5 1.9 fusion.102
  70.6 6.2 %all-to-all-start.3 = ((bf16[16,128,64]{1,2,0:T(8,128)(2,1)}), bf16[16,128,64]{1,2,0:T(8,128)(2,1)S(1)}, u32[]{:S(2)}, u32[]{:S(2)}) async-start(bf16[16,128,64]{1,2,0:T(8,128)(2,1)} %copy.86), calls=%async_computation.3 | async-start | bytes 524288 | tf_op jit(solution)/shard_map/all_to_all | solution.py:166
  77.1 7.2 %all-to-all-done.3 = bf16[16,128,64]{1,2,0:T(8,128)(2,1)S(1)} async-done(((bf16[16,128,64]{1,2,0:T(8,128)(2,1)}), bf16[16,128,64]{1,2,0:T(8,128)(2,1)S(1)}, u32[]{:S(2)}, u32[]{:S(2)}) %all-to-all-start.3) | async-done | bytes 262176 | tf_op jit(solution)/shard_map/all_to_all | solution.py:166
  84.7 3.0 %fusion.73 = (f32[128]{0:T(128)S(1)}, f32[128,2048]{1,0:T(8,128)S(1)}) fusion(bf16[128,1024]{0,1:T(8,128)(2,1)S(1)} %fusion.30, bf16[1024,2048]{1,0:T(8,128)(2,1)} %param.29, bf16[1,128,2048]{2,1,0:T(8,128)(2,1)S(1)} %copy-done.4), kind=kOutput, calls=%fused_computation.132 | convolution fusion | flops 537919360 | bytes 6029824 | tf_op jit(solution)/shard_map/dot_general | solution.py:168
  88.3 2.6 %convolution_convert_fusion.1 = bf16[768,2048]{1,0:T(8,128)(2,1)} fusion(pred[768,128]{1,0:T(8,128)(4,1)S(1)} %fusion.20, bf16[128,2048]{1,0:T(8,128)(2,1)S(1)} %add_convert_fusion.1), kind=kOutput, calls=%fused_computation.15 | convolution fusion | flops 404226048 | bytes 3768320 | tf_op jit(solution)/shard_map/dot_general | solution.py:181
  91.0 6.3 %reshape.250 = bf16[128,6,2048]{2,1,0:T(8,128)(2,1)} reshape(bf16[768,2048]{1,0:T(8,128)(2,1)} %convolution_convert_fusion.1) | data formatting | bytes 6291456 | tf_op jit(solution)/shard_map/reshape | solution.py:183
  97.2 62.2 %all_to_all.60 = bf16[128,6,2048]{2,1,0:T(8,128)(2,1)} all-to-all(bf16[128,6,2048]{2,1,0:T(8,128)(2,1)} %reshape.250), channel_id=1, replica_groups=mesh['sp'=16,'dp'=8] {'sp','dp'}, dimensions={0} | all-to-all | bytes 6291456 | tf_op jit(solution)/shard_map/all_to_all | solution.py:182
  159.4 6.3 %reshape.251 = bf16[768,2048]{1,0:T(8,128)(2,1)} reshape(bf16[128,6,2048]{2,1,0:T(8,128)(2,1)} %all_to_all.60) | data formatting | bytes 6291456 | tf_op jit(solution)/shard_map/reshape | solution.py:185
  165.7 5.5 %fusion.18 = f32[768,512]{1,0:T(8,128)} fusion(bf16[768,2048]{1,0:T(8,128)(2,1)} %reshape.251, bf16[1,2048,512]{2,1,0:T(8,128)(2,1)} %param.34), kind=kOutput, calls=%fused_computation.30 | convolution fusion | flops 1610612736 | bytes 6815744 | tf_op jit(solution)/shard_map/dot_general | solution.py:94
  171.2 8.2 %convolution_convert_fusion = bf16[768,2048]{1,0:T(8,128)(2,1)} fusion(bf16[1,512,2048]{2,1,0:T(8,128)(2,1)S(1)} %copy-done, f32[768,512]{1,0:T(8,128)} %fusion.18, bf16[768,2048]{1,0:T(8,128)(2,1)} %reshape.251, bf16[1,2048,512]{2,1,0:T(8,128)(2,1)} %param.35), kind=kOutput, calls=%fused_computation.14 | convolution fusion | flops 3225157632 | bytes 12058624 | tf_op jit(solution)/shard_map/dot_general | solution.py:97
  179.4 6.3 %reshape.252 = bf16[128,6,2048]{2,1,0:T(8,128)(2,1)} reshape(bf16[768,2048]{1,0:T(8,128)(2,1)} %convolution_convert_fusion) | data formatting | bytes 6291456 | tf_op jit(solution)/shard_map/reshape | solution.py:189
  185.7 5.6 %all-to-all-start.5 = ((bf16[128,6,2048]{2,1,0:T(8,128)(2,1)}), bf16[128,6,2048]{2,1,0:T(8,128)(2,1)}, u32[]{:S(2)}, u32[]{:S(2)}) async-start(bf16[128,6,2048]{2,1,0:T(8,128)(2,1)} %reshape.252), calls=%async_computation.5 | async-start | bytes 8388608 | tf_op jit(solution)/shard_map/all_to_all | solution.py:191
  191.7 2.0 fusion.75
  193.8 4.1 %fusion.25 = f32[128,2048]{1,0:T(8,128)} fusion(bf16[512,2048]{1,0:T(8,128)(2,1)} %param.39, bf16[128,2048]{1,0:T(8,128)(2,1)S(1)} %add_convert_fusion.1, bf16[2048,512]{1,0:T(8,128)(2,1)} %param.38, f32[128,512]{1,0:T(8,128)S(1)} %fusion.75), kind=kOutput, calls=%fused_computation.38 | convolution fusion | flops 537264128 | bytes 6029312 | tf_op jit(solution)/shard_map/dot_general | solution.py:97
  197.9 46.1 %all-to-all-done.5 = bf16[128,6,2048]{2,1,0:T(8,128)(2,1)} async-done(((bf16[128,6,2048]{2,1,0:T(8,128)(2,1)}), bf16[128,6,2048]{2,1,0:T(8,128)(2,1)}, u32[]{:S(2)}, u32[]{:S(2)}) %all-to-all-start.5) | async-done | bytes 3145760 | tf_op jit(solution)/shard_map/all_to_all | solution.py:191
  244.0 6.3 %reshape.253 = bf16[768,2048]{1,0:T(8,128)(2,1)} reshape(bf16[128,6,2048]{2,1,0:T(8,128)(2,1)} %all-to-all-done.5) | data formatting | bytes 6291456 | tf_op jit(solution)/shard_map/reshape | solution.py:192
  250.4 2.6 %convolution_multiply_fusion.2 = f32[128,2048]{1,0:T(8,128)S(1)} fusion(bf16[768,2048]{1,0:T(8,128)(2,1)} %reshape.253, f32[128]{0:T(128)S(1)} %get-tuple-element.99, s32[128]{0:T(128)S(1)} %get-tuple-element.75), kind=kOutput, calls=%fused_computation.18 | convolution fusion | flops 403013632 | bytes 4195328 | tf_op jit(solution)/shard_map/dot_general | solution.py:198
  255.1 1.1 fusion.74
  (109 shorter events, 27.9 us)
Async XLA Ops:
  0.0 171.2 %copy-start = (bf16[1,512,2048]{2,1,0:T(8,128)(2,1)S(1)}, bf16[1,512,2048]{2,1,0:T(8,128)(2,1)}, u32[]{:S(2)}) copy-start(bf16[1,512,2048]{2,1,0:T(8,128)(2,1)} %param.36) | copy-start | bytes 6291460
  1.7 16.1 %all-to-all-start.2 = ((bf16[16,128,32]{1,2,0:T(8,128)(2,1)}), bf16[16,128,32]{1,2,0:T(8,128)(2,1)S(1)}, u32[]{:S(2)}, u32[]{:S(2)}) async-start(bf16[16,128,32]{1,2,0:T(8,128)(2,1)} %broadcast_in_dim.10), calls=%async_computation.2 | async-start | bytes 262144 | tf_op jit(solution)/shard_map/all_to_all | solution.py:23
  17.7 15.3 %all-to-all-start = ((bf16[128,16,96]{0,2,1:T(8,128)(2,1)}), bf16[128,16,96]{0,2,1:T(8,128)(2,1)S(1)}, u32[]{:S(2)}, u32[]{:S(2)}) async-start(bf16[128,16,96]{0,2,1:T(8,128)(2,1)} %bitcast.1), calls=%async_computation | async-start | bytes 786432 | tf_op jit(solution)/shard_map/all_to_all | solution.py:140
  33.1 0.7 copy-start.3
  33.8 12.9 %all-to-all-start.1 = ((bf16[128,16,128]{2,0,1:T(8,128)(2,1)}), bf16[128,16,128]{2,0,1:T(8,128)(2,1)S(1)}, u32[]{:S(2)}, u32[]{:S(2)}) async-start(bf16[128,16,128]{2,0,1:T(8,128)(2,1)} %bitcast.135), calls=%async_computation.1 | async-start | bytes 1048576 | tf_op jit(solution)/shard_map/all_to_all | solution.py:141
  43.6 4.4 %copy-start.7 = (bf16[4,512,64]{1,2,0:T(8,128)(2,1)S(1)}, bf16[4,512,64]{1,2,0:T(8,128)(2,1)}, u32[]{:S(2)}) copy-start(bf16[4,512,64]{1,2,0:T(8,128)(2,1)} %custom-call) | copy-start | bytes 786436
  48.0 28.8 %copy-start.6 = (s32[1,128,4]{2,1,0:T(8,128)S(1)}, s32[1,128,4]{2,1,0:T(8,128)}, u32[]{:S(2)}) copy-start(s32[1,128,4]{2,1,0:T(8,128)} %reduce_sum.92) | copy-start | bytes 6148
  48.0 36.5 %copy-start.13 = (f32[1024]{0:T(1024)S(1)}, f32[1024]{0:T(1024)}, u32[]{:S(2)}) copy-start(f32[1024]{0:T(1024)} %param.28) | copy-start | bytes 12292
  51.3 1.0 copy-start.5
  56.6 1.0 copy-start.5
  62.0 1.0 copy-start.5
  67.4 1.0 copy-start.5
  69.5 15.2 %copy-start.4 = (bf16[1,128,2048]{2,1,0:T(8,128)(2,1)S(1)}, bf16[1,128,2048]{2,1,0:T(8,128)(2,1)}, u32[]{:S(2)}) copy-start(bf16[1,128,2048]{2,1,0:T(8,128)(2,1)} %param.22) | copy-start | bytes 1572868
  70.6 13.7 %all-to-all-start.3 = ((bf16[16,128,64]{1,2,0:T(8,128)(2,1)}), bf16[16,128,64]{1,2,0:T(8,128)(2,1)S(1)}, u32[]{:S(2)}, u32[]{:S(2)}) async-start(bf16[16,128,64]{1,2,0:T(8,128)(2,1)} %copy.86), calls=%async_computation.3 | async-start | bytes 524288 | tf_op jit(solution)/shard_map/all_to_all | solution.py:166
  84.7 3.3 %copy-start.8 = (f32[2048]{0:T(1024)S(1)}, f32[2048]{0:T(1024)}, u32[]{:S(2)}) copy-start(f32[2048]{0:T(1024)} %param.31) | copy-start | bytes 24580
  84.7 3.3 %copy-start.9 = (f32[2048]{0:T(1024)S(1)}, f32[2048]{0:T(1024)}, u32[]{:S(2)}) copy-start(f32[2048]{0:T(1024)} %param.30) | copy-start | bytes 24580
  185.7 5.8 %copy-start.12 = (f32[1,128,4]{1,2,0:T(4,128)S(1)}, f32[1,128,4]{1,2,0:T(4,128)}, u32[]{:S(2)}) copy-start(f32[1,128,4]{1,2,0:T(4,128)} %param.33) | copy-start | bytes 6148
  185.7 58.4 %all-to-all-start.5 = ((bf16[128,6,2048]{2,1,0:T(8,128)(2,1)}), bf16[128,6,2048]{2,1,0:T(8,128)(2,1)}, u32[]{:S(2)}, u32[]{:S(2)}) async-start(bf16[128,6,2048]{2,1,0:T(8,128)(2,1)} %reshape.252), calls=%async_computation.5 | async-start | bytes 8388608 | tf_op jit(solution)/shard_map/all_to_all | solution.py:191
  250.4 2.8 %copy-start.1 = (bf16[768,2048]{1,0:T(8,128)(2,1)S(1)}, bf16[768,2048]{1,0:T(8,128)(2,1)}, u32[]{:S(2)}) copy-start(bf16[768,2048]{1,0:T(8,128)(2,1)} %reshape.253) | copy-start | bytes 9437188
  253.9 1.2 copy-start.2
  255.1 1.4 copy-start.10
  255.1 1.4 copy-start.11
where the time goes:
time: 259 us; the launch traced here: 258 us
  blocking collectives  62.2 us (24%)
  waiting for transfers between devices  61.1 us (24%)
  matrix products  44.5 us (17%)
  local copies, waits for them, and re-layouts  43.8 us (17%)
  starting transfers between devices  30.6 us (12%)
  other arithmetic  12 us (5%)
  loops' own time  2.94 us (1%)
    all_to_all x1, blocking collectives, per_device(): lax.all_to_all(outbound.reshape(group, capacity, D), ('sp', 'dp'), split_...  62.2 us
    all_to_all x1, waiting for transfers between devices, per_device(): lax.all_to_all(produced, ('sp', 'dp'), split_axis=0, concat_axis=0, tiled...  46.1 us
    dot_general x2, matrix products, swiglu_rows(): return jnp.dot(inner, down_mat, preferred_element_type=jnp.float32)  12.4 us
    all_to_all x1, starting transfers between devices, copy_for_each(): lax.all_to_all(jnp.broadcast_to(value[None], (size, *value.shape)), axis,...  8.59 us
    dot_general x2, matrix products, swiglu_rows(): gated = jnp.dot(rows, gate_mat, preferred_element_type=jnp.float32)  7.5 us
    dot_general x4, matrix products, one_block(): jnp.dot(query_rows, key_full.T, preferred_element_type=jnp.float32) * factor  7.42 us
    all_to_all x1, waiting for transfers between devices, per_device(): lax.all_to_all(query_send, 'sp', split_axis=1, concat_axis=0, tiled=True)  7.35 us
    all_to_all x1, waiting for transfers between devices, per_device(): lax.all_to_all(outgoing, 'sp', split_axis=0, concat_axis=2, tiled=True)  7.21 us
  transfers between devices with their start and end apart: 5, of which 4 were waited for; matrix products, arithmetic and copies ran while one was open for 9% of the time, Pallas kernels for 0%

commit v1 on v0

--- a/solution.py
+++ b/solution.py
@@ -3,6 +3,8 @@
 import jax
 import jax.numpy as jnp
 from jax import lax
+from jax.experimental import pallas as pl
+from jax.experimental.pallas import tpu as pltpu
 from jax.sharding import PartitionSpec as P
 
 D = 2048
@@ -90,11 +92,263 @@
     return attended.reshape(length, values.shape[1])
 
 
-def swiglu_rows(rows, gate_mat, up_mat, down_mat):
-    gated = jnp.dot(rows, gate_mat, preferred_element_type=jnp.float32)
-    lifted = jnp.dot(rows, up_mat, preferred_element_type=jnp.float32)
-    inner = (jax.nn.silu(gated) * lifted).astype(jnp.bfloat16)
-    return jnp.dot(inner, down_mat, preferred_element_type=jnp.float32)
+MESH = pl.DeviceIdType.MESH
+GROUPS = 8
+PER_GROUP = 16
+SLOTS = 6
+GROUP_ROWS = PER_GROUP * SLOTS
+TILES = D // 128
+
+
+def position_of(sp, dp):
+    return sp // 4, sp % 4, dp // 2, dp % 2
+
+
+def step_of(k):
+    dc, dy, dx = (k // 16) % 2, (k // 4) % 4, k % 4
+    return (k // 32 + 8 - dx - dy) % 4, dy, dx, dc
+
+
+def device_at(here, k, sign):
+    z, y, x, c = here
+    dz, dy, dx, dc = step_of(k)
+    z, y = (z + 4 + sign * dz) % 4, (y + 4 + sign * dy) % 4
+    x, c = (x + 4 + sign * dx) % 4, (c + dc) % 2
+    return (z * 4 + y, x * 2 + c)
+
+
+def order_of(expert_ids, here):
+    z, y, x, c = here
+    ez, ey, ex, ec = expert_ids // 32, (expert_ids // 8) % 4, (expert_ids // 2) % 4, expert_ids % 2
+    dz, dy, dx, dc = (ez - z) & 3, (ey - y) & 3, (ex - x) & 3, (ec + c) & 1
+    return (((dz + dy + dx) & 3) * 2 + dc) * 16 + dy * 4 + dx
+
+
+def iota(shape, dim):
+    return lax.broadcasted_iota(jnp.int32, shape, dim)
+
+
+def experts_kernel(
+    ids_ref, ids_t_ref, weights_ref, attended_ref, attn_gain_ref, hidden_ref,
+    gain1_ref, bias1_ref, gain2_ref, bias2_ref,
+    out_proj_hbm, gate_hbm, up_hbm, down_hbm, sgate_hbm, sup_hbm, sdown_hbm,
+    out_ref,
+    out_proj, gate, up, down, sgate, sup, sdown,
+    first, places_t, places, gates, send, arrived, made, returned, flat, rows, total,
+    load_sem, send_sem, recv_sem, back_sem, ret_sem,
+):
+    here = position_of(lax.axis_index("sp"), lax.axis_index("dp"))
+    loads = [
+        pltpu.make_async_copy(src, dst, load_sem.at[i])
+        for i, (src, dst) in enumerate(
+            (
+                (out_proj_hbm, out_proj), (sgate_hbm, sgate), (sup_hbm, sup), (sdown_hbm, sdown),
+                (gate_hbm.at[0], gate), (up_hbm.at[0], up), (down_hbm.at[0], down),
+            )
+        )
+    ]
+    for load in loads:
+        load.start()
+    barrier = pltpu.get_barrier_semaphore()
+
+    def greet(k, carry):
+        pl.semaphore_signal(barrier, inc=1, device_id=device_at(here, k, 1), device_id_type=MESH)
+        return carry
+
+    lax.fori_loop(1, 128, greet, 0)
+
+    ids_t = ids_t_ref[...]
+    named_t = jnp.zeros((128, 128), jnp.bool_)
+    for col in range(TOP_K):
+        named_t = named_t | (iota((128, 128), 0) == ids_t[col : col + 1, :])
+    before = (iota((128, 128), 0) < iota((128, 128), 1)).astype(jnp.bfloat16)
+    count_t = jnp.dot(named_t.astype(jnp.bfloat16), before, preferred_element_type=jnp.float32)
+    order_t = order_of(ids_t, here)
+    for col in range(TOP_K):
+        slot = jnp.sum(
+            jnp.where(iota((128, 128), 0) == ids_t[col : col + 1, :], count_t, 0.0),
+            axis=0, keepdims=True,
+        )
+        places_t[col : col + 1, :] = order_t[col : col + 1, :] * SLOTS + slot.astype(jnp.int32)
+    ids = ids_ref[...]
+    named = jnp.zeros((128, 128), jnp.bool_)
+    for col in range(TOP_K):
+        named = named | (iota((128, 128), 1) == ids[:, col : col + 1])
+    after = (iota((128, 128), 1) < iota((128, 128), 0)).astype(jnp.bfloat16)
+    count = jnp.dot(after, named.astype(jnp.bfloat16), preferred_element_type=jnp.float32)
+    order = order_of(ids, here)
+    for col in range(TOP_K):
+        slot = jnp.sum(
+            jnp.where(iota((128, 128), 1) == ids[:, col : col + 1], count, 0.0),
+            axis=1, keepdims=True,
+        )
+        places[:, col : col + 1] = order[:, col : col + 1] * SLOTS + slot.astype(jnp.int32)
+    weights = weights_ref[...]
+    gates[...] = weights / jnp.sum(weights, axis=-1, keepdims=True) * ROUTED
+
+    attn_normed = rms_scaled(attended_ref[...], attn_gain_ref[...]).astype(jnp.bfloat16)
+    loads[0].wait()
+    mixed = jnp.dot(attn_normed, out_proj[...], preferred_element_type=jnp.float32)
+    first[...] = layer_norm(
+        ALPHA * hidden_ref[...].astype(jnp.float32) + mixed, gain1_ref[...], bias1_ref[...]
+    ).astype(jnp.bfloat16)
+
+    def pack(group, source, target):
+        for tile in range(TILES):
+            flat[pl.ds(tile, GROUP_ROWS, stride=TILES), :] = source[:, tile * 128 : tile * 128 + 128]
+        target[pl.ds(group * PER_GROUP, PER_GROUP)] = (
+            flat[...].astype(jnp.bfloat16).reshape(PER_GROUP, SLOTS * TILES, 128)
+        )
+
+    def unpack(group, source):
+        flat[...] = (
+            source[pl.ds(group * PER_GROUP, PER_GROUP)]
+            .reshape(GROUP_ROWS * TILES, 128)
+            .astype(jnp.float32)
+        )
+        for tile in range(TILES):
+            rows[:, tile * 128 : tile * 128 + 128] = flat[
+                pl.ds(tile, GROUP_ROWS, stride=TILES), :
+            ].astype(jnp.bfloat16)
+
+    def dispatch(k, carry):
+        pltpu.make_async_remote_copy(
+            send.at[k], arrived.at[k], send_sem, recv_sem.at[k // PER_GROUP],
+            device_id=device_at(here, k, 1), device_id_type=MESH,
+        ).start()
+        return carry
+
+    def reply(k, carry):
+        pltpu.make_async_remote_copy(
+            made.at[k], returned.at[k], back_sem, ret_sem.at[k // PER_GROUP],
+            device_id=device_at(here, k, -1), device_id_type=MESH,
+        ).start()
+        return carry
+
+    def wait_blocks(group, buffer, sem):
+        @pl.when(group == 0)
+        def _():
+            block = buffer.at[pl.ds(0, PER_GROUP - 1)]
+            pltpu.make_async_copy(block, block, sem.at[group]).wait()
+
+        @pl.when(group > 0)
+        def _():
+            block = buffer.at[pl.ds(0, PER_GROUP)]
+            pltpu.make_async_copy(block, block, sem.at[group]).wait()
+
+    def load_group(group, carry):
+        picks = iota((GROUP_ROWS, 128), 0) + group * GROUP_ROWS
+        chosen = jnp.zeros((GROUP_ROWS, 128), jnp.bool_)
+        for col in range(TOP_K):
+            chosen = chosen | (picks == places_t[col : col + 1, :])
+        out = jnp.dot(
+            chosen.astype(jnp.bfloat16), first[...], preferred_element_type=jnp.float32
+        )
+        pack(group, out, send)
+
+        @pl.when(group == 0)
+        def _():
+            pl.semaphore_wait(barrier, 127)
+
+        lax.fori_loop(jnp.maximum(group * PER_GROUP, 1), (group + 1) * PER_GROUP, dispatch, 0)
+        return carry
+
+    lax.fori_loop(0, GROUPS, load_group, 0)
+    arrived[0] = send[0]
+
+    for load in loads[1:4]:
+        load.wait()
+    tokens = first[...]
+    gated = jnp.dot(tokens, sgate[...], preferred_element_type=jnp.float32)
+    lifted = jnp.dot(tokens, sup[...], preferred_element_type=jnp.float32)
+    inner = (gated / (1.0 + jnp.exp(-gated)) * lifted).astype(jnp.bfloat16)
+    total[...] = ALPHA * tokens.astype(jnp.float32) + jnp.dot(
+        inner, sdown[...], preferred_element_type=jnp.float32
+    )
+    for load in loads[4:]:
+        load.wait()
+
+    def expert_group(group, carry):
+        wait_blocks(group, arrived, recv_sem)
+        unpack(group, arrived)
+        tokens = rows[...]
+        gated = jnp.dot(tokens, gate[...], preferred_element_type=jnp.float32)
+        lifted = jnp.dot(tokens, up[...], preferred_element_type=jnp.float32)
+        inner = (gated / (1.0 + jnp.exp(-gated)) * lifted).astype(jnp.bfloat16)
+        out = jnp.dot(inner, down[...], preferred_element_type=jnp.float32)
+        pack(group, out, made)
+        lax.fori_loop(jnp.maximum(group * PER_GROUP, 1), (group + 1) * PER_GROUP, reply, 0)
+        return carry
+
+    lax.fori_loop(0, GROUPS, expert_group, 0)
+    returned[0] = made[0]
+
+    def combine_group(group, carry):
+        wait_blocks(group, returned, ret_sem)
+        unpack(group, returned)
+        picks = iota((128, GROUP_ROWS), 1) + group * GROUP_ROWS
+        share = jnp.zeros((128, GROUP_ROWS), jnp.float32)
+        for col in range(TOP_K):
+            share = share + jnp.where(
+                picks == places[:, col : col + 1], gates[:, col : col + 1], 0.0
+            )
+        high = share.astype(jnp.bfloat16)
+        low = (share - high.astype(jnp.float32)).astype(jnp.bfloat16)
+        tokens = rows[...]
+        total[...] += jnp.dot(high, tokens, preferred_element_type=jnp.float32) + jnp.dot(
+            low, tokens, preferred_element_type=jnp.float32
+        )
+        return carry
+
+    lax.fori_loop(0, GROUPS, combine_group, 0)
+    out_ref[...] = layer_norm(total[...], gain2_ref[...], bias2_ref[...]).astype(jnp.bfloat16)
+    sent = send.at[pl.ds(0, 127)]
+    pltpu.make_async_copy(sent, sent, send_sem).wait()
+    pltpu.make_async_copy(sent, sent, back_sem).wait()
+
+
+def experts_layer(
+    ids, ids_t, weights, attended, attn_gain, hidden, gain1, bias1, gain2, bias2,
+    out_proj, gate_proj, up_proj, down_proj, shared_gate, shared_up, shared_down,
+):
+    bf16, f32 = jnp.bfloat16, jnp.float32
+    vmem = pl.BlockSpec(memory_space=pltpu.VMEM)
+    hbm = pl.BlockSpec(memory_space=pl.ANY)
+    blocks = pltpu.VMEM((GROUPS * PER_GROUP, SLOTS * TILES, 128), bf16)
+    return pl.pallas_call(
+        experts_kernel,
+        out_shape=jax.ShapeDtypeStruct((128, D), bf16),
+        in_specs=[vmem] * 10 + [hbm] * 7,
+        out_specs=vmem,
+        scratch_shapes=[
+            pltpu.VMEM((1024, D), bf16),
+            pltpu.VMEM((D, 512), bf16),
+            pltpu.VMEM((D, 512), bf16),
+            pltpu.VMEM((512, D), bf16),
+            pltpu.VMEM((D, 512), bf16),
+            pltpu.VMEM((D, 512), bf16),
+            pltpu.VMEM((512, D), bf16),
+            pltpu.VMEM((128, D), bf16),
+            pltpu.VMEM((TOP_K, 128), jnp.int32),
+            pltpu.VMEM((128, TOP_K), jnp.int32),
+            pltpu.VMEM((128, TOP_K), f32),
+            blocks, blocks, blocks, blocks,
+            pltpu.VMEM((GROUP_ROWS * TILES, 128), f32),
+            pltpu.VMEM((GROUP_ROWS, D), bf16),
+            pltpu.VMEM((128, D), f32),
+            pltpu.SemaphoreType.DMA((7,)),
+            pltpu.SemaphoreType.DMA,
+            pltpu.SemaphoreType.DMA((GROUPS,)),
+            pltpu.SemaphoreType.DMA,
+            pltpu.SemaphoreType.DMA((GROUPS,)),
+        ],
+        compiler_params=pltpu.CompilerParams(
+            collective_id=1, has_side_effects=True, vmem_limit_bytes=56 * 2**20
+        ),
+    )(
+        ids, ids_t, weights, attended, attn_gain, hidden, gain1, bias1, gain2, bias2,
+        out_proj, gate_proj, up_proj, down_proj, shared_gate, shared_up, shared_down,
+    )
 
 
 def per_device(
@@ -164,42 +418,11 @@
         seq_devices, tok_rows, heads_here * VALUE_HEAD_WIDTH
     )
     incoming = lax.all_to_all(outgoing, "sp", split_axis=0, concat_axis=2, tiled=True)
-    attn_normed = rms_scaled(incoming[0], attn_gain).astype(jnp.bfloat16)
-    mixed = jnp.dot(attn_normed, out_proj, preferred_element_type=jnp.float32)
-    first = layer_norm(
-        ALPHA * hidden_in[0].astype(jnp.float32) + mixed, norm1_gain, norm1_bias
-    ).astype(jnp.bfloat16)
-    group = lax.axis_size("sp") * lax.axis_size("dp")
-    capacity = (tok_rows * TOP_K * 3 + 2 * group - 1) // (2 * group)
-    entries = expert_ids[0].reshape(-1)
-    onehot = (entries[:, None] == jnp.arange(group, dtype=jnp.int32)[None, :]).astype(jnp.int32)
-    earlier = jnp.cumsum(onehot, axis=0) - onehot
-    slots = jnp.sum(earlier * onehot, axis=-1)
-    places = (entries * capacity + slots).reshape(tok_rows, TOP_K)
-    slot_ids = jnp.arange(group * capacity, dtype=jnp.int32)
-    dispatch = jnp.any(places[None, :, :] == slot_ids[:, None, None], axis=-1).astype(jnp.bfloat16)
-    outbound = jnp.dot(dispatch, first, preferred_element_type=jnp.float32).astype(jnp.bfloat16)
-    arrived = lax.all_to_all(
-        outbound.reshape(group, capacity, D), ("sp", "dp"), split_axis=0, concat_axis=0, tiled=True
-    )
-    flat_rows = arrived.reshape(group * capacity, D)
-    produced = (
-        swiglu_rows(flat_rows, gate_proj[0], up_proj[0], down_proj[0])
-        .astype(jnp.bfloat16)
-        .reshape(group, capacity, D)
-    )
-    returned = lax.all_to_all(produced, ("sp", "dp"), split_axis=0, concat_axis=0, tiled=True)
-    returned_flat = returned.reshape(group * capacity, D)
-    weights = route_weights[0]
-    gates = weights / jnp.sum(weights, axis=-1, keepdims=True) * ROUTED
-    routed = jnp.zeros((tok_rows, D), jnp.float32)
-    for column in range(TOP_K):
-        picker = (places[:, column : column + 1] == slot_ids[None, :]).astype(jnp.bfloat16)
-        picked = jnp.dot(picker, returned_flat, preferred_element_type=jnp.float32)
-        routed = routed + gates[:, column : column + 1] * picked
-    feed = routed + swiglu_rows(first, shared_gate, shared_up, shared_down)
-    result = layer_norm(ALPHA * first.astype(jnp.float32) + feed, norm2_gain, norm2_bias).astype(
-        jnp.bfloat16
+    ids = expert_ids[0]
+    result = experts_layer(
+        ids, ids.T, route_weights[0], incoming[0], attn_gain[None], hidden_in[0],
+        norm1_gain[None], norm1_bias[None], norm2_gain[None], norm2_bias[None],
+        out_proj, gate_proj, up_proj, down_proj, shared_gate, shared_up, shared_down,
     )
     return result.reshape(1, tok_rows, D)
 

time: 259 us -> 172 us (0.66)
  Pallas kernels: 0 us -> 91.3 us
  blocking collectives: 62.2 us -> 0 us
  waiting for transfers between devices: 61.1 us -> 18.4 us
  matrix products: 44.5 us -> 13.3 us
  local copies, waits for them, and re-layouts: 43.8 us -> 15.6 us
  starting transfers between devices: 30.6 us -> 19.7 us
  other arithmetic: 12 us -> 8.43 us
    pallas_call x0 -> x1, Pallas kernels: none -> 91.3 us  [experts_layer(): pl.pallas_call(experts_kernel, out_shape=jax.ShapeDtypeStruct((128, D), b...]
    all_to_all x1 -> x0, blocking collectives: 62.2 us -> none  [per_device(): lax.all_to_all(outbound.reshape(group, capacity, D), ('sp', 'dp'), split_...]
    all_to_all x1 -> x0, waiting for transfers between devices: 46.1 us -> none  [per_device(): lax.all_to_all(produced, ('sp', 'dp'), split_axis=0, concat_axis=0, tiled...]
    dot_general x10 -> x0, matrix products: 30.6 us -> none  [the longest x2 12.4 us: swiglu_rows(): return jnp.dot(inner, down_mat, preferred_element_type=jnp.float32)]
    reshape x4 -> x0, local copies, waits for them, and re-layouts: 25.2 us -> none  [the longest x1 6.34 us: per_device(): flat_rows = arrived.reshape(group * capacity, D)]
    all_to_all x1 -> x0, starting transfers between devices: 5.63 us -> none  [per_device(): lax.all_to_all(produced, ('sp', 'dp'), split_axis=0, concat_axis=0, tiled...]
    all_to_all x1, waiting for transfers between devices: 0.01 us -> 3.94 us  [copy_for_each(): lax.all_to_all(jnp.broadcast_to(value[None], (size, *value.shape)), axis,...]
    all_to_all x1, starting transfers between devices: 6.67 us -> 3.55 us  [per_device(): lax.all_to_all(query_send, 'sp', split_axis=1, concat_axis=0, tiled=True)]
  transfers between devices with their start and end apart: 5 -> 4, of which waited for: 4 -> 4; matrix products, arithmetic and copies ran while one was open for 9% -> 8% of each run, Pallas kernels for 0% -> 0%
where the time goes in v1:
time: 172 us; the launch traced here: 170 us
  Pallas kernels  91.3 us (53%)
  starting transfers between devices  19.7 us (11%)
  waiting for transfers between devices  18.4 us (11%)
  local copies, waits for them, and re-layouts  15.6 us (9%)
  matrix products  13.3 us (8%)
  other arithmetic  8.43 us (5%)
  loops' own time  2.74 us (2%)
    pallas_call x1, Pallas kernels, experts_layer(): pl.pallas_call(experts_kernel, out_shape=jax.ShapeDtypeStruct((128, D), b...  91.3 us
    all_to_all x1, starting transfers between devices, copy_for_each(): lax.all_to_all(jnp.broadcast_to(value[None], (size, *value.shape)), axis,...  8.59 us
    dot_general x4, matrix products, one_block(): jnp.dot(query_rows, key_full.T, preferred_element_type=jnp.float32) * factor  7.64 us
    all_to_all x1, waiting for transfers between devices, per_device(): lax.all_to_all(outgoing, 'sp', split_axis=0, concat_axis=2, tiled=True)  6.06 us
    all_to_all x1, waiting for transfers between devices, per_device(): lax.all_to_all(query_send, 'sp', split_axis=1, concat_axis=0, tiled=True)  5.8 us
    unnamed x11, local copies, waits for them, and re-layouts  4.54 us
    dot_general x4, matrix products, one_block(): jnp.dot(weights, values, preferred_element_type=jnp.float32)  4.3 us
    all_to_all x1, starting transfers between devices, per_device(): lax.all_to_all(outgoing, 'sp', split_axis=0, concat_axis=2, tiled=True)  4.03 us
  transfers between devices with their start and end apart: 4, of which 4 were waited for; matrix products, arithmetic and copies ran while one was open for 8% of the time, Pallas kernels for 0%

profile of v1, /device:TPU:1, one launch (start us, length us, event | category | flops | bytes accessed | tf_op | source)
XLA Modules:
  0.0 169.7 jit_solution(6993661569639385295)
XLA Ops:
  0.0 0.8 bitcast_convert_fusion
  1.7 8.6 %all-to-all-start.2 = ((bf16[16,128,32]{1,2,0:T(8,128)(2,1)}), bf16[16,128,32]{1,2,0:T(8,128)(2,1)S(1)}, u32[]{:S(2)}, u32[]{:S(2)}) async-start(bf16[16,128,32]{1,2,0:T(8,128)(2,1)} %broadcast_in_dim.27), calls=%async_computation.2 | async-start | bytes 262144 | tf_op jit(solution)/shard_map/all_to_all | solution.py:25
  10.3 1.9 %copy.58 = bf16[1,128,1536]{1,2,0:T(8,128)(2,1)} copy(bf16[1,128,1536]{2,1,0:T(8,128)(2,1)} %param.23) | data formatting | bytes 786432 | tf_op args[1]
  12.2 1.0 fusion.11
  13.2 3.9 %all-to-all-done.2 = bf16[16,128,32]{1,2,0:T(8,128)(2,1)S(1)} async-done(((bf16[16,128,32]{1,2,0:T(8,128)(2,1)}), bf16[16,128,32]{1,2,0:T(8,128)(2,1)S(1)}, u32[]{:S(2)}, u32[]{:S(2)}) %all-to-all-start.2) | async-done | bytes 131104 | tf_op jit(solution)/shard_map/all_to_all | solution.py:25
  17.1 3.6 %all-to-all-start = ((bf16[128,16,96]{0,2,1:T(8,128)(2,1)}), bf16[128,16,96]{0,2,1:T(8,128)(2,1)S(1)}, u32[]{:S(2)}, u32[]{:S(2)}) async-start(bf16[128,16,96]{0,2,1:T(8,128)(2,1)} %bitcast.3), calls=%async_computation | async-start | bytes 786432 | tf_op jit(solution)/shard_map/all_to_all | solution.py:394
  20.7 1.4 fusion.10
  22.1 0.9 copy.79
  23.3 5.8 %all-to-all-done = bf16[128,16,96]{0,2,1:T(8,128)(2,1)S(1)} async-done(((bf16[128,16,96]{0,2,1:T(8,128)(2,1)}), bf16[128,16,96]{0,2,1:T(8,128)(2,1)S(1)}, u32[]{:S(2)}, u32[]{:S(2)}) %all-to-all-start) | async-done | bytes 393248 | tf_op jit(solution)/shard_map/all_to_all | solution.py:394
  29.1 3.6 %all-to-all-start.1 = ((bf16[128,16,128]{2,0,1:T(8,128)(2,1)}), bf16[128,16,128]{2,0,1:T(8,128)(2,1)S(1)}, u32[]{:S(2)}, u32[]{:S(2)}) async-start(bf16[128,16,128]{2,0,1:T(8,128)(2,1)} %bitcast.80), calls=%async_computation.1 | async-start | bytes 1048576 | tf_op jit(solution)/shard_map/all_to_all | solution.py:395
  33.4 1.0 copy.71
  34.4 1.0 copy.72
  35.4 1.0 copy.70
  36.4 2.7 %pad_maximum_fusion = bf16[4,512,96]{2,1,0:T(8,128)(2,1)} fusion(bf16[4,512,16]{2,1,0:T(8,128)(2,1)} %bitcast.82, bf16[4,512,16]{2,1,0:T(8,128)(2,1)} %bitcast.81, bf16[4,512,64]{2,1,0:T(8,128)(2,1)} %bitcast.83), kind=kLoop, calls=%fused_computation.18 | loop fusion | flops 1179648 | bytes 786432 | tf_op jit(solution)/shard_map/concatenate | solution.py:404
  39.1 2.6 %all-to-all-done.1 = bf16[128,16,128]{2,0,1:T(8,128)(2,1)S(1)} async-done(((bf16[128,16,128]{2,0,1:T(8,128)(2,1)}), bf16[128,16,128]{2,0,1:T(8,128)(2,1)S(1)}, u32[]{:S(2)}, u32[]{:S(2)}) %all-to-all-start.1) | async-done | bytes 524320 | tf_op jit(solution)/shard_map/all_to_all | solution.py:395
  41.7 1.0 slice_bitcast_fusion
  43.0 20.0 %while.18 = (s32[]{:T(128)}, bf16[4,512,64]{1,2,0:T(8,128)(2,1)S(1)}, s32[4]{0:T(128)S(1)}, bf16[4,512,96]{2,1,0:T(8,128)(2,1)}, bf16[2048,96]{1,0:T(8,128)(2,1)...) while((s32[]{:T(128)}, bf16[4,512,64]{1,2,0:T(8,128)(2,1)S(1)}, s32[4]{0:T(128)S(1)}, ...), condition=%wide.region_4.5_spmd.clone, body=%wide.region_1.4_spmd.clone.sunk | while | flops 345013760 | bytes 14760593 | solution.py:91
  44.3 1.9 %fusion.46 = (f32[512]{0:T(512)S(1)}, f32[512,2048]{1,0:T(8,128)S(1)}) fusion(bf16[2048,96]{1,0:T(8,128)(2,1)S(1)} %get-tuple-element.153, bf16[4,512,96]{2,1,0:T(8,128)(2,1)} %get-tuple-element.152, s32[]{:T(128)} %get-tuple-element.141, s32[512]{0:T(512)S(1)} %iota_add_fusion.2), kind=kOutput, calls=%fused_computation.56.clone.1 | convolution fusion | flops 205520384 | bytes 4723200 | tf_op jit(solution)/shard_map/while/body/eval_jaxpr/while/body/eval_jaxpr/dot_general | solution.py:83
  46.9 1.1 fusion.48
  49.3 1.9 %fusion.46 = (f32[512]{0:T(512)S(1)}, f32[512,2048]{1,0:T(8,128)S(1)}) fusion(bf16[2048,96]{1,0:T(8,128)(2,1)S(1)} %get-tuple-element.153, bf16[4,512,96]{2,1,0:T(8,128)(2,1)} %get-tuple-element.152, s32[]{:T(128)} %get-tuple-element.141, s32[512]{0:T(512)S(1)} %iota_add_fusion.2), kind=kOutput, calls=%fused_computation.56.clone.1 | convolution fusion | flops 205520384 | bytes 4723200 | tf_op jit(solution)/shard_map/while/body/eval_jaxpr/while/body/eval_jaxpr/dot_general | solution.py:83
  51.9 1.1 fusion.48
  54.3 1.9 %fusion.46 = (f32[512]{0:T(512)S(1)}, f32[512,2048]{1,0:T(8,128)S(1)}) fusion(bf16[2048,96]{1,0:T(8,128)(2,1)S(1)} %get-tuple-element.153, bf16[4,512,96]{2,1,0:T(8,128)(2,1)} %get-tuple-element.152, s32[]{:T(128)} %get-tuple-element.141, s32[512]{0:T(512)S(1)} %iota_add_fusion.2), kind=kOutput, calls=%fused_computation.56.clone.1 | convolution fusion | flops 205520384 | bytes 4723200 | tf_op jit(solution)/shard_map/while/body/eval_jaxpr/while/body/eval_jaxpr/dot_general | solution.py:83
  56.9 1.1 fusion.48
  59.3 1.9 %fusion.46 = (f32[512]{0:T(512)S(1)}, f32[512,2048]{1,0:T(8,128)S(1)}) fusion(bf16[2048,96]{1,0:T(8,128)(2,1)S(1)} %get-tuple-element.153, bf16[4,512,96]{2,1,0:T(8,128)(2,1)} %get-tuple-element.152, s32[]{:T(128)} %get-tuple-element.141, s32[512]{0:T(512)S(1)} %iota_add_fusion.2), kind=kOutput, calls=%fused_computation.56.clone.1 | convolution fusion | flops 205520384 | bytes 4723200 | tf_op jit(solution)/shard_map/while/body/eval_jaxpr/while/body/eval_jaxpr/dot_general | solution.py:83
  61.9 1.1 fusion.48
  63.4 0.8 copy.67
  64.1 4.0 %all-to-all-start.3 = ((bf16[16,128,64]{1,2,0:T(8,128)(2,1)}), bf16[16,128,64]{1,2,0:T(8,128)(2,1)S(1)}, u32[]{:S(2)}, u32[]{:S(2)}) async-start(bf16[16,128,64]{1,2,0:T(8,128)(2,1)} %copy.67), calls=%async_computation.3 | async-start | bytes 524288 | tf_op jit(solution)/shard_map/all_to_all | solution.py:420
  68.9 0.7 copy.68.ids_ref
  69.6 6.1 %all-to-all-done.3 = bf16[16,128,64]{1,2,0:T(8,128)(2,1)S(1)} async-done(((bf16[16,128,64]{1,2,0:T(8,128)(2,1)}), bf16[16,128,64]{1,2,0:T(8,128)(2,1)S(1)}, u32[]{:S(2)}, u32[]{:S(2)}) %all-to-all-start.3) | async-done | bytes 262176 | tf_op jit(solution)/shard_map/all_to_all | solution.py:420
  75.7 0.8 copy.69.attended_ref
  76.6 91.3 %shard_map.190 = bf16[128,2048]{1,0:T(8,128)(2,1)} custom-call(s32[128,4]{1,0:T(8,128)} %copy.68.ids_ref, s32[4,128]{1,0:T(4,128)} %bitcast.92, f32[128,4]{1,0:T(8,128)} %bitcast.87, bf16[128,1024]{1,0:T(8,128)(2,1)} %copy.69.attended_ref, f32[1,1024]{1,0:T(1,128)} %bitcast.94, bf16[128,2048]{1,0:T(8,128)(2,1)} %bitcast.86, f32[1,2048]{1,0:T(1,128)} %bitcast.88, ...), custom_call_target="tpu_custom_call" | custom-call | tf_op jit(solution)/shard_map/pallas_call | solution.py:318
  167.8 1.9 %copy.90 = bf16[1,128,2048]{2,1,0:T(8,128)(2,1)} copy(bf16[1,128,2048]{2,1,0:T(8,128)(2,1)} %bitcast.84) | data formatting | bytes 1048576
  (46 shorter events, 8.4 us)
Async XLA Ops:
  0.0 20.7 %copy-start = (bf16[512,2048]{1,0:T(8,128)(2,1)S(1)}, bf16[512,2048]{1,0:T(8,128)(2,1)}, u32[]{:S(2)}) copy-start(bf16[512,2048]{1,0:T(8,128)(2,1)} %param.27) | copy-start | bytes 6291460
  1.7 15.5 %all-to-all-start.2 = ((bf16[16,128,32]{1,2,0:T(8,128)(2,1)}), bf16[16,128,32]{1,2,0:T(8,128)(2,1)S(1)}, u32[]{:S(2)}, u32[]{:S(2)}) async-start(bf16[16,128,32]{1,2,0:T(8,128)(2,1)} %broadcast_in_dim.27), calls=%async_computation.2 | async-start | bytes 262144 | tf_op jit(solution)/shard_map/all_to_all | solution.py:25
  17.1 12.0 %all-to-all-start = ((bf16[128,16,96]{0,2,1:T(8,128)(2,1)}), bf16[128,16,96]{0,2,1:T(8,128)(2,1)S(1)}, u32[]{:S(2)}, u32[]{:S(2)}) async-start(bf16[128,16,96]{0,2,1:T(8,128)(2,1)} %bitcast.3), calls=%async_computation | async-start | bytes 786432 | tf_op jit(solution)/shard_map/all_to_all | solution.py:394
  29.1 12.5 %all-to-all-start.1 = ((bf16[128,16,128]{2,0,1:T(8,128)(2,1)}), bf16[128,16,128]{2,0,1:T(8,128)(2,1)S(1)}, u32[]{:S(2)}, u32[]{:S(2)}) async-start(bf16[128,16,128]{2,0,1:T(8,128)(2,1)} %bitcast.80), calls=%async_computation.1 | async-start | bytes 1048576 | tf_op jit(solution)/shard_map/all_to_all | solution.py:395
  36.4 6.6 %copy-start.2 = (bf16[4,512,64]{1,2,0:T(8,128)(2,1)S(1)}, bf16[4,512,64]{1,2,0:T(8,128)(2,1)}, u32[]{:S(2)}) copy-start(bf16[4,512,64]{1,2,0:T(8,128)(2,1)} %custom-call) | copy-start | bytes 786436
  43.0 25.2 %copy-start.4 = (f32[1,128,4]{1,2,0:T(4,128)S(1)}, f32[1,128,4]{1,2,0:T(4,128)}, u32[]{:S(2)}) copy-start(f32[1,128,4]{1,2,0:T(4,128)} %param.33) | copy-start | bytes 6148
  43.0 25.9 %copy-start.3 = (s32[1,128,4]{1,2,0:T(4,128)S(1)}, s32[1,128,4]{1,2,0:T(4,128)}, u32[]{:S(2)}) copy-start(s32[1,128,4]{1,2,0:T(4,128)} %param.32) | copy-start | bytes 6148
  44.3 2.6 %copy-start.1 = (bf16[2048,64]{1,0:T(8,128)(2,1)S(1)}, bf16[2048,64]{1,0:T(8,128)(2,1)}, u32[]{:S(2)}) copy-start(bf16[2048,64]{1,0:T(8,128)(2,1)} %get-tuple-element.154) | copy-start | bytes 786436 | tf_op jit(solution)/shard_map/while/body/eval_jaxpr/while
  49.3 2.6 %copy-start.1 = (bf16[2048,64]{1,0:T(8,128)(2,1)S(1)}, bf16[2048,64]{1,0:T(8,128)(2,1)}, u32[]{:S(2)}) copy-start(bf16[2048,64]{1,0:T(8,128)(2,1)} %get-tuple-element.154) | copy-start | bytes 786436 | tf_op jit(solution)/shard_map/while/body/eval_jaxpr/while
  54.3 2.6 %copy-start.1 = (bf16[2048,64]{1,0:T(8,128)(2,1)S(1)}, bf16[2048,64]{1,0:T(8,128)(2,1)}, u32[]{:S(2)}) copy-start(bf16[2048,64]{1,0:T(8,128)(2,1)} %get-tuple-element.154) | copy-start | bytes 786436 | tf_op jit(solution)/shard_map/while/body/eval_jaxpr/while
  59.3 2.6 %copy-start.1 = (bf16[2048,64]{1,0:T(8,128)(2,1)S(1)}, bf16[2048,64]{1,0:T(8,128)(2,1)}, u32[]{:S(2)}) copy-start(bf16[2048,64]{1,0:T(8,128)(2,1)} %get-tuple-element.154) | copy-start | bytes 786436 | tf_op jit(solution)/shard_map/while/body/eval_jaxpr/while
  64.1 11.6 %all-to-all-start.3 = ((bf16[16,128,64]{1,2,0:T(8,128)(2,1)}), bf16[16,128,64]{1,2,0:T(8,128)(2,1)S(1)}, u32[]{:S(2)}, u32[]{:S(2)}) async-start(bf16[16,128,64]{1,2,0:T(8,128)(2,1)} %copy.67), calls=%async_computation.3 | async-start | bytes 524288 | tf_op jit(solution)/shard_map/all_to_all | solution.py:420

commit v2 on v1

--- a/solution.py
+++ b/solution.py
@@ -2,6 +2,7 @@
 
 import jax
 import jax.numpy as jnp
+import numpy as np
 from jax import lax
 from jax.experimental import pallas as pl
 from jax.experimental.pallas import tpu as pltpu
@@ -20,24 +21,6 @@
 THETA = 10000.0
 
 
-def copy_for_each(value, axis):
-    size = lax.axis_size(axis)
-    return lax.all_to_all(
-        jnp.broadcast_to(value[None], (size, *value.shape)), axis, 0, 0, tiled=True
-    )
-
-
-def in_order(tiles, dim):
-    lengths = list(tiles.shape[1:])
-    lengths[dim] *= tiles.shape[0]
-    return jnp.moveaxis(tiles, 0, dim).reshape(lengths)
-
-
-def collect(value, axis, dim):
-    tiles = copy_for_each(value, axis)
-    return in_order(tiles, dim)
-
-
 def rms_scaled(values, scaling):
     widened = values.astype(jnp.float32)
     return (
@@ -51,45 +34,11 @@
     return centre * lax.rsqrt(spread + 1e-05) * scaling + bias_add
 
 
-def rotation_tables(positions, rot_width):
-    frequency = THETA ** (-jnp.arange(0, rot_width, 2, dtype=jnp.float32) / rot_width)
-    angles = positions.astype(jnp.float32)[:, None] * frequency[None, :]
-    return (jnp.cos(angles), jnp.sin(angles))
-
-
-def turn(values, cosine_table, sine_table):
-    half_width = values.shape[-1] // 2
-    first_half = values[..., :half_width]
-    second_half = values[..., half_width:]
-    return jnp.concatenate(
-        [
-            first_half * cosine_table - second_half * sine_table,
-            second_half * cosine_table + first_half * sine_table,
-        ],
-        axis=-1,
-    )
-
-
-def attend(query, key_full, values):
-    length = query.shape[0]
-    span_rows = 512
-    block_count = length // span_rows
-    blocks = query.reshape(block_count, span_rows, query.shape[1])
-    key_pos = jnp.arange(length, dtype=jnp.int32)
-    factor = 1.0 / math.sqrt(query.shape[1])
-
-    def one_block(inputs):
-        block_index, query_rows = inputs
-        scores = jnp.dot(query_rows, key_full.T, preferred_element_type=jnp.float32) * factor
-        query_pos = block_index * span_rows + jnp.arange(span_rows, dtype=jnp.int32)
-        scores = jnp.where(key_pos[None, :] <= query_pos[:, None], scores, -jnp.inf)
-        row_max = jnp.max(scores, axis=-1, keepdims=True)
-        weights = jnp.exp(scores - row_max)
-        weights = (weights / jnp.sum(weights, axis=-1, keepdims=True)).astype(jnp.bfloat16)
-        return jnp.dot(weights, values, preferred_element_type=jnp.float32).astype(jnp.bfloat16)
-
-    attended = lax.map(one_block, (jnp.arange(block_count, dtype=jnp.int32), blocks))
-    return attended.reshape(length, values.shape[1])
+def rotation_tables(devices, rows):
+    frequency = np.power(THETA, -np.arange(0, QK_ROPE, 2) / QK_ROPE).astype(np.float32)
+    positions = np.arange(devices * rows, dtype=np.float32).reshape(devices, 1, rows)
+    angles = (positions * frequency[None, :, None]).astype(np.float64)
+    return np.concatenate([np.cos(angles), np.sin(angles)], axis=1).astype(np.float32)
 
 
 MESH = pl.DeviceIdType.MESH
@@ -109,6 +58,12 @@
     return (k // 32 + 8 - dx - dy) % 4, dy, dx, dc
 
 
+def peer_at(here, k):
+    z, y = here[:2]
+    dy = k % 4
+    return (z + (k // 4 + 4 - dy)) % 4 * 4 + (y + dy) % 4
+
+
 def device_at(here, k, sign):
     z, y, x, c = here
     dz, dy, dx, dc = step_of(k)
@@ -128,21 +83,28 @@
     return lax.broadcasted_iota(jnp.int32, shape, dim)
 
 
-def experts_kernel(
-    ids_ref, ids_t_ref, weights_ref, attended_ref, attn_gain_ref, hidden_ref,
+def layer_kernel(
+    ids_ref, ids_t_ref, weights_ref, rope_ref, latent_gain_ref, attn_gain_ref,
     gain1_ref, bias1_ref, gain2_ref, bias2_ref,
+    latent_hbm, latent_up_hbm, queries_hbm, tables_hbm, hidden_hbm,
     out_proj_hbm, gate_hbm, up_hbm, down_hbm, sgate_hbm, sup_hbm, sdown_hbm,
     out_ref,
+    latent, latent_up, queries, tables, hidden,
     out_proj, gate, up, down, sgate, sup, sdown,
+    turned, message, letters, keys, asked, values_t, scores, heads_out, heads_in,
     first, places_t, places, gates, send, arrived, made, returned, flat, rows, total,
-    load_sem, send_sem, recv_sem, back_sem, ret_sem,
+    load_sem, msg_sem, letter_sem, head_sem, heads_sem,
+    send_sem, recv_sem, back_sem, ret_sem,
 ):
-    here = position_of(lax.axis_index("sp"), lax.axis_index("dp"))
+    sp, dp = lax.axis_index("sp"), lax.axis_index("dp")
+    here = position_of(sp, dp)
     loads = [
         pltpu.make_async_copy(src, dst, load_sem.at[i])
         for i, (src, dst) in enumerate(
             (
-                (out_proj_hbm, out_proj), (sgate_hbm, sgate), (sup_hbm, sup), (sdown_hbm, sdown),
+                (latent_hbm, latent), (latent_up_hbm, latent_up), (queries_hbm, queries),
+                (tables_hbm.at[sp], tables), (hidden_hbm, hidden), (out_proj_hbm, out_proj),
+                (sgate_hbm, sgate), (sup_hbm, sup), (sdown_hbm, sdown),
                 (gate_hbm.at[0], gate), (up_hbm.at[0], up), (down_hbm.at[0], down),
             )
         )
@@ -156,6 +118,48 @@
         return carry
 
     lax.fori_loop(1, 128, greet, 0)
+
+    loads[3].wait()
+    cosine, sine = tables[0:16, :], tables[16:32, :]
+
+    def turn(both):
+        a, b = both[0:16].astype(jnp.float32), both[16:32].astype(jnp.float32)
+        return jnp.concatenate([a * cosine - b * sine, b * cosine + a * sine], axis=0).astype(
+            jnp.bfloat16
+        )
+
+    rope = jnp.concatenate(
+        [rope_ref[...].astype(jnp.float32), jnp.zeros((128, 96), jnp.float32)], axis=1
+    )
+    rope_t = turn(rope.T[0:32])
+    loads[2].wait()
+    for tile in range(12):
+        turned[tile * 128 : tile * 128 + 128, :] = queries[:, tile * 128 : tile * 128 + 128].T
+    for head in range(16):
+        block = turned[head * 96 : head * 96 + 96, :]
+        message[head, 0:64, :] = block[0:64]
+        message[head, 64:96, :] = turn(block[64:96])
+        message[head, 96:128, :] = rope_t
+    loads[0].wait()
+    normed = rms_scaled(latent[...], latent_gain_ref[...]).astype(jnp.bfloat16)
+    loads[1].wait()
+    keys_values = jnp.dot(normed, latent_up[...], preferred_element_type=jnp.float32).astype(
+        jnp.bfloat16
+    )
+    for head in range(16):
+        message[head, 128:256, :] = keys_values[:, head * 128 : head * 128 + 128]
+    pl.semaphore_wait(barrier, 127)
+
+    def deliver(k, carry):
+        peer = peer_at(here, k)
+        pltpu.make_async_remote_copy(
+            message.at[peer], letters.at[sp], msg_sem, letter_sem,
+            device_id=(peer, dp), device_id_type=MESH,
+        ).start()
+        return carry
+
+    lax.fori_loop(1, 16, deliver, 0)
+    letters[sp] = message[sp]
 
     ids_t = ids_t_ref[...]
     named_t = jnp.zeros((128, 128), jnp.bool_)
@@ -186,11 +190,76 @@
     weights = weights_ref[...]
     gates[...] = weights / jnp.sum(weights, axis=-1, keepdims=True) * ROUTED
 
-    attn_normed = rms_scaled(attended_ref[...], attn_gain_ref[...]).astype(jnp.bfloat16)
-    loads[0].wait()
+    asked[...] = jnp.zeros_like(asked)
+    fifteen = message.at[pl.ds(0, 15)]
+    pltpu.make_async_copy(fifteen, fifteen, letter_sem).wait()
+    for block in range(16):
+        span = slice(block * 128, block * 128 + 128)
+        top, pair = letters[block, 0:128, :], letters[block, 128:256, :]
+        keys[span, 0:128] = pair
+        keys[span, 128:256] = top.T
+        asked[0:64, span] = top[0:64]
+        asked[224:256, span] = top[64:96]
+        values_t[:, span] = pair.T
+
+    factor = math.log2(math.e) / math.sqrt(PLAIN_HEAD_WIDTH + QK_ROPE)
+
+    def attend(index):
+        asking = asked[:, index * 256 : index * 256 + 256]
+        peak = None
+        for other in range(index + 1):
+            span = slice(other * 256, other * 256 + 256)
+            part = jnp.dot(keys[span, :], asking, preferred_element_type=jnp.float32)
+            if other == index:
+                part = jnp.where(iota((256, 256), 0) <= iota((256, 256), 1), part, -jnp.inf)
+            scores[span, :] = part
+            high = jnp.max(part, axis=0, keepdims=True)
+            peak = high if peak is None else jnp.maximum(peak, high)
+        peak = peak * factor
+        weight, mixed = 0.0, 0.0
+        for other in range(index + 1):
+            span = slice(other * 256, other * 256 + 256)
+            part = jnp.exp2(scores[span, :] * factor - peak)
+            weight = weight + jnp.sum(part, axis=0, keepdims=True)
+            mixed = mixed + jnp.dot(
+                values_t[64:128, span], part.astype(jnp.bfloat16),
+                preferred_element_type=jnp.float32,
+            )
+        mixed = (mixed / weight).astype(jnp.bfloat16)
+        heads_out[2 * index] = mixed[:, 0:128]
+        heads_out[2 * index + 1] = mixed[:, 128:256]
+
+    def give_back(base):
+        def give(k, carry):
+            peer = base + (sp + k) % 8
+
+            @pl.when(peer != sp)
+            def _():
+                pltpu.make_async_remote_copy(
+                    heads_out.at[peer], heads_in.at[sp], head_sem, heads_sem,
+                    device_id=(peer, dp), device_id_type=MESH,
+                ).start()
+
+            return carry
+
+        lax.fori_loop(0, 8, give, 0)
+
+    for index in (7, 6, 5, 4):
+        attend(index)
+    give_back(8)
+    for index in (3, 2, 1, 0):
+        attend(index)
+    give_back(0)
+    heads_in[sp] = heads_out[sp]
+    loads[4].wait()
+    loads[5].wait()
+    arrivals = heads_out.at[pl.ds(0, 15)]
+    pltpu.make_async_copy(arrivals, arrivals, heads_sem).wait()
+    attended = heads_in[...].reshape(1024, 128).T
+    attn_normed = rms_scaled(attended, attn_gain_ref[...]).astype(jnp.bfloat16)
     mixed = jnp.dot(attn_normed, out_proj[...], preferred_element_type=jnp.float32)
     first[...] = layer_norm(
-        ALPHA * hidden_ref[...].astype(jnp.float32) + mixed, gain1_ref[...], bias1_ref[...]
+        ALPHA * hidden[...].astype(jnp.float32) + mixed, gain1_ref[...], bias1_ref[...]
     ).astype(jnp.bfloat16)
 
     def pack(group, source, target):
@@ -246,17 +315,13 @@
         )
         pack(group, out, send)
 
-        @pl.when(group == 0)
-        def _():
-            pl.semaphore_wait(barrier, 127)
-
         lax.fori_loop(jnp.maximum(group * PER_GROUP, 1), (group + 1) * PER_GROUP, dispatch, 0)
         return carry
 
     lax.fori_loop(0, GROUPS, load_group, 0)
     arrived[0] = send[0]
 
-    for load in loads[1:4]:
+    for load in loads[6:9]:
         load.wait()
     tokens = first[...]
     gated = jnp.dot(tokens, sgate[...], preferred_element_type=jnp.float32)
@@ -265,7 +330,7 @@
     total[...] = ALPHA * tokens.astype(jnp.float32) + jnp.dot(
         inner, sdown[...], preferred_element_type=jnp.float32
     )
-    for load in loads[4:]:
+    for load in loads[9:]:
         load.wait()
 
     def expert_group(group, carry):
@@ -305,22 +370,32 @@
     sent = send.at[pl.ds(0, 127)]
     pltpu.make_async_copy(sent, sent, send_sem).wait()
     pltpu.make_async_copy(sent, sent, back_sem).wait()
-
-
-def experts_layer(
-    ids, ids_t, weights, attended, attn_gain, hidden, gain1, bias1, gain2, bias2,
-    out_proj, gate_proj, up_proj, down_proj, shared_gate, shared_up, shared_down,
+    pltpu.make_async_copy(fifteen, fifteen, msg_sem).wait()
+    pltpu.make_async_copy(arrivals, arrivals, head_sem).wait()
+
+
+def per_device(
+    hidden_in, queries, key_value_latent, keys_rope, latent_norm_gain, latent_up_weight,
+    attn_gain, out_proj, norm1_gain, norm1_bias, expert_ids, route_weights,
+    gate_proj, up_proj, down_proj, shared_gate, shared_up, shared_down, norm2_gain, norm2_bias,
 ):
     bf16, f32 = jnp.bfloat16, jnp.float32
     vmem = pl.BlockSpec(memory_space=pltpu.VMEM)
     hbm = pl.BlockSpec(memory_space=pl.ANY)
     blocks = pltpu.VMEM((GROUPS * PER_GROUP, SLOTS * TILES, 128), bf16)
-    return pl.pallas_call(
-        experts_kernel,
+    tables = jnp.asarray(rotation_tables(16, 128))
+    ids = expert_ids[0]
+    result = pl.pallas_call(
+        layer_kernel,
         out_shape=jax.ShapeDtypeStruct((128, D), bf16),
-        in_specs=[vmem] * 10 + [hbm] * 7,
+        in_specs=[vmem] * 10 + [hbm] * 12,
         out_specs=vmem,
         scratch_shapes=[
+            pltpu.VMEM((128, 512), bf16),
+            pltpu.VMEM((512, 2048), bf16),
+            pltpu.VMEM((128, 1536), bf16),
+            pltpu.VMEM((32, 128), f32),
+            pltpu.VMEM((128, D), bf16),
             pltpu.VMEM((1024, D), bf16),
             pltpu.VMEM((D, 512), bf16),
             pltpu.VMEM((D, 512), bf16),
@@ -328,6 +403,15 @@
             pltpu.VMEM((D, 512), bf16),
             pltpu.VMEM((D, 512), bf16),
             pltpu.VMEM((512, D), bf16),
+            pltpu.VMEM((1536, 128), bf16),
+            pltpu.VMEM((16, 256, 128), bf16),
+            pltpu.VMEM((16, 256, 128), bf16),
+            pltpu.VMEM((2048, 256), bf16),
+            pltpu.VMEM((256, 2048), bf16),
+            pltpu.VMEM((128, 2048), bf16),
+            pltpu.VMEM((2048, 256), f32),
+            pltpu.VMEM((16, 64, 128), bf16),
+            pltpu.VMEM((16, 64, 128), bf16),
             pltpu.VMEM((128, D), bf16),
             pltpu.VMEM((TOP_K, 128), jnp.int32),
             pltpu.VMEM((128, TOP_K), jnp.int32),
@@ -336,95 +420,26 @@
             pltpu.VMEM((GROUP_ROWS * TILES, 128), f32),
             pltpu.VMEM((GROUP_ROWS, D), bf16),
             pltpu.VMEM((128, D), f32),
-            pltpu.SemaphoreType.DMA((7,)),
+            pltpu.SemaphoreType.DMA((12,)),
+            pltpu.SemaphoreType.DMA,
+            pltpu.SemaphoreType.DMA,
+            pltpu.SemaphoreType.DMA,
+            pltpu.SemaphoreType.DMA,
             pltpu.SemaphoreType.DMA,
             pltpu.SemaphoreType.DMA((GROUPS,)),
             pltpu.SemaphoreType.DMA,
             pltpu.SemaphoreType.DMA((GROUPS,)),
         ],
         compiler_params=pltpu.CompilerParams(
-            collective_id=1, has_side_effects=True, vmem_limit_bytes=56 * 2**20
+            collective_id=1, has_side_effects=True, vmem_limit_bytes=58 * 2**20
         ),
     )(
-        ids, ids_t, weights, attended, attn_gain, hidden, gain1, bias1, gain2, bias2,
+        ids, ids.T, route_weights[0], keys_rope[0], latent_norm_gain[None], attn_gain[None],
+        norm1_gain[None], norm1_bias[None], norm2_gain[None], norm2_bias[None],
+        key_value_latent[0], latent_up_weight, queries[0], tables, hidden_in[0],
         out_proj, gate_proj, up_proj, down_proj, shared_gate, shared_up, shared_down,
     )
-
-
-def per_device(
-    hidden_in,
-    queries,
-    key_value_latent,
-    keys_rope,
-    latent_norm_gain,
-    latent_up_weight,
-    attn_gain,
-    out_proj,
-    norm1_gain,
-    norm1_bias,
-    expert_ids,
-    route_weights,
-    gate_proj,
-    up_proj,
-    down_proj,
-    shared_gate,
-    shared_up,
-    shared_down,
-    norm2_gain,
-    norm2_bias,
-):
-    seq_devices = lax.axis_size("sp")
-    tok_rows = hidden_in.shape[1]
-    length = tok_rows * seq_devices
-    heads_here = ATTENTION_HEADS // seq_devices
-    normed = rms_scaled(key_value_latent[0], latent_norm_gain).astype(jnp.bfloat16)
-    keys_values = jnp.dot(normed, latent_up_weight, preferred_element_type=jnp.float32).astype(
-        jnp.bfloat16
-    )
-    local_pos = lax.axis_index("sp") * tok_rows + jnp.arange(tok_rows, dtype=jnp.int32)
-    cos_local, sin_local = rotation_tables(local_pos, QK_ROPE)
-    keys_turned = turn(keys_rope[0].astype(jnp.float32), cos_local, sin_local).astype(jnp.bfloat16)
-    query_send = queries[0].reshape(
-        tok_rows, seq_devices, heads_here * (PLAIN_HEAD_WIDTH + QK_ROPE)
-    )
-    pair_send = keys_values.reshape(
-        tok_rows, seq_devices, heads_here * (PLAIN_HEAD_WIDTH + VALUE_HEAD_WIDTH)
-    )
-    query_heads, pair_heads = (
-        lax.all_to_all(query_send, "sp", split_axis=1, concat_axis=0, tiled=True),
-        lax.all_to_all(pair_send, "sp", split_axis=1, concat_axis=0, tiled=True),
-    )
-    keys_whole = collect(keys_turned, "sp", 0)
-    cos_whole, sin_whole = rotation_tables(jnp.arange(length, dtype=jnp.int32), QK_ROPE)
-    query_turned = turn(
-        query_heads[..., PLAIN_HEAD_WIDTH:].astype(jnp.float32),
-        cos_whole[:, None, :],
-        sin_whole[:, None, :],
-    ).astype(jnp.bfloat16)
-    query_full = jnp.concatenate([query_heads[..., :PLAIN_HEAD_WIDTH], query_turned], axis=-1)
-    key_full = jnp.concatenate(
-        [pair_heads[..., :PLAIN_HEAD_WIDTH], keys_whole[:, None, :]], axis=-1
-    )
-    values_heads = pair_heads[..., PLAIN_HEAD_WIDTH:]
-    by_head = lax.map(
-        lambda inputs: attend(inputs[0], inputs[1], inputs[2]),
-        (
-            jnp.moveaxis(query_full, 1, 0),
-            jnp.moveaxis(key_full, 1, 0),
-            jnp.moveaxis(values_heads, 1, 0),
-        ),
-    )
-    outgoing = jnp.moveaxis(by_head, 0, 1).reshape(
-        seq_devices, tok_rows, heads_here * VALUE_HEAD_WIDTH
-    )
-    incoming = lax.all_to_all(outgoing, "sp", split_axis=0, concat_axis=2, tiled=True)
-    ids = expert_ids[0]
-    result = experts_layer(
-        ids, ids.T, route_weights[0], incoming[0], attn_gain[None], hidden_in[0],
-        norm1_gain[None], norm1_bias[None], norm2_gain[None], norm2_bias[None],
-        out_proj, gate_proj, up_proj, down_proj, shared_gate, shared_up, shared_down,
-    )
-    return result.reshape(1, tok_rows, D)
+    return result[None]
 
 
 def solution(mesh):

time: 172 us -> 125 us (0.73)
  Pallas kernels: 91.3 us -> 117 us
  starting transfers between devices: 19.7 us -> 0 us
  waiting for transfers between devices: 18.4 us -> 0 us
  matrix products: 13.3 us -> 0 us
  local copies, waits for them, and re-layouts: 15.6 us -> 6.1 us
  other arithmetic: 8.43 us -> 0 us
  loops' own time: 2.74 us -> 0 us
    pallas_call x1, Pallas kernels: 91.3 us -> 117 us  [per_device(): pl.pallas_call(layer_kernel, out_shape=jax.ShapeDtypeStruct((128, D), bf1...]
    all_to_all x4 -> x0, starting transfers between devices: 19.7 us -> none  [the longest x1 8.59 us: copy_for_each(): lax.all_to_all(jnp.broadcast_to(value[None], (size, *value.shape)), axis,...]
    all_to_all x4 -> x0, waiting for transfers between devices: 18.4 us -> none  [the longest x1 6.06 us: per_device(): lax.all_to_all(outgoing, 'sp', split_axis=0, concat_axis=2, tiled=True)]
    dot_general x9 -> x0, matrix products: 13.3 us -> none  [the longest x4 7.64 us: one_block(): jnp.dot(query_rows, key_full.T, preferred_element_type=jnp.float32) * factor]
    reduce_sum x5 -> x0, other arithmetic: 3.86 us -> none  [the longest x4 2.84 us: one_block(): jnp.sum(weights, axis=-1, keepdims=True)]
    concatenate x3 -> x0, local copies, waits for them, and re-layouts: 3.03 us -> none  [the longest x2 2.04 us: turn(): jnp.concatenate([first_half * cosine_table - second_half * sine_table, se...]
    another operation x1 -> x0, loops' own time: 2.74 us -> none  [attend(): lax.map(one_block, (jnp.arange(block_count, dtype=jnp.int32), blocks))]
    concatenate x2 -> x0, other arithmetic: 2.69 us -> none  [the longest x1 2.68 us: per_device(): jnp.concatenate([query_heads[..., :PLAIN_HEAD_WIDTH], query_turned], axis...]
  transfers between devices with their start and end apart: 4 -> 0, of which waited for: 4 -> 0; matrix products, arithmetic and copies ran while one was open for 8% -> 0% of each run, Pallas kernels for 0% -> 0%
where the time goes in v2:
time: 125 us; the launch traced here: 123 us
  Pallas kernels  117 us (94%)
  local copies, waits for them, and re-layouts  6.1 us (5%)
    pallas_call x1, Pallas kernels, per_device(): pl.pallas_call(layer_kernel, out_shape=jax.ShapeDtypeStruct((128, D), bf1...  117 us
    unnamed x3, local copies, waits for them, and re-layouts  4.69 us

profile of v2, /device:TPU:1, one launch (start us, length us, event | category | flops | bytes accessed | tf_op | source)
XLA Modules:
  0.0 123.4 jit_solution(2523964119870103008)
XLA Ops:
  0.0 1.4 %copy.23 = bf16[1,128,32]{2,1,0:T(8,128)(2,1)} copy(bf16[1,128,32]{1,2,0:T(8,128)(2,1)} %param.24) | data formatting | bytes 16384 | tf_op args[3]
  1.4 1.4 %copy.22 = f32[1,128,4]{2,1,0:T(8,128)} copy(f32[1,128,4]{1,2,0:T(4,128)} %param.32) | data formatting | bytes 4096 | tf_op args[11]
  2.8 1.4 %copy.24.ids_ref = s32[128,4]{1,0:T(8,128)} copy(s32[128,4]{0,1:T(4,128)} %bitcast.25) | data formatting | bytes 4096 | tf_op jit(solution)/shard_map/squeeze | solution.py:387
  4.2 117.3 %shard_map.199 = bf16[128,2048]{1,0:T(8,128)(2,1)} custom-call(s32[128,4]{1,0:T(8,128)} %copy.24.ids_ref, s32[4,128]{1,0:T(4,128)} %bitcast.26, f32[128,4]{1,0:T(8,128)} %bitcast.18, bf16[128,32]{1,0:T(8,128)(2,1)} %bitcast.20, f32[1,512]{1,0:T(1,128)} %bitcast.28, f32[1,1024]{1,0:T(1,128)} %bitcast.27, f32[1,2048]{1,0:T(1,128)} %bitcast.21, ...), custom_call_target="tpu_custom_call" | custom-call | tf_op jit(solution)/shard_map/pallas_call | solution.py:388
  121.5 1.9 %copy.26 = bf16[1,128,2048]{2,1,0:T(8,128)(2,1)} copy(bf16[1,128,2048]{2,1,0:T(8,128)(2,1)} %bitcast.15) | data formatting | bytes 1048576

commit v3 on v2

--- a/solution.py
+++ b/solution.py
@@ -84,16 +84,18 @@
 
 
 def layer_kernel(
-    ids_ref, ids_t_ref, weights_ref, rope_ref, latent_gain_ref, attn_gain_ref,
-    gain1_ref, bias1_ref, gain2_ref, bias2_ref,
+    ids_t_hbm, weights_t_hbm, rope_t_hbm, latent_gain_hbm, attn_gain_hbm,
+    gain1_hbm, bias1_hbm, gain2_hbm, bias2_hbm,
     latent_hbm, latent_up_hbm, queries_hbm, tables_hbm, hidden_hbm,
     out_proj_hbm, gate_hbm, up_hbm, down_hbm, sgate_hbm, sup_hbm, sdown_hbm,
     out_ref,
+    ids_t_ref, weights_t_ref, rope_t_ref, latent_gain_ref, attn_gain_ref,
+    gain1_ref, bias1_ref, gain2_ref, bias2_ref,
     latent, latent_up, queries, tables, hidden,
     out_proj, gate, up, down, sgate, sup, sdown,
     turned, message, letters, keys, asked, values_t, scores, heads_out, heads_in,
     first, places_t, places, gates, send, arrived, made, returned, flat, rows, total,
-    load_sem, msg_sem, letter_sem, head_sem, heads_sem,
+    load_sem, msg_sem, letter_sem, value_sem, head_sem, heads_sem,
     send_sem, recv_sem, back_sem, ret_sem,
 ):
     sp, dp = lax.axis_index("sp"), lax.axis_index("dp")
@@ -106,11 +108,15 @@
                 (tables_hbm.at[sp], tables), (hidden_hbm, hidden), (out_proj_hbm, out_proj),
                 (sgate_hbm, sgate), (sup_hbm, sup), (sdown_hbm, sdown),
                 (gate_hbm.at[0], gate), (up_hbm.at[0], up), (down_hbm.at[0], down),
+                (latent_gain_hbm, latent_gain_ref), (rope_t_hbm, rope_t_ref),
+                (ids_t_hbm, ids_t_ref), (weights_t_hbm, weights_t_ref),
+                (attn_gain_hbm, attn_gain_ref), (gain1_hbm, gain1_ref), (bias1_hbm, bias1_ref),
+                (gain2_hbm, gain2_ref), (bias2_hbm, bias2_ref),
             )
         )
     ]
-    for load in loads:
-        load.start()
+    for i in (3, 13, 2, 0, 12, 1):
+        loads[i].start()
     barrier = pltpu.get_barrier_semaphore()
 
     def greet(k, carry):
@@ -120,6 +126,7 @@
     lax.fori_loop(1, 128, greet, 0)
 
     loads[3].wait()
+    loads[13].wait()
     cosine, sine = tables[0:16, :], tables[16:32, :]
 
     def turn(both):
@@ -128,10 +135,7 @@
             jnp.bfloat16
         )
 
-    rope = jnp.concatenate(
-        [rope_ref[...].astype(jnp.float32), jnp.zeros((128, 96), jnp.float32)], axis=1
-    )
-    rope_t = turn(rope.T[0:32])
+    rope_t = turn(rope_t_ref[...])
     loads[2].wait()
     for tile in range(12):
         turned[tile * 128 : tile * 128 + 128, :] = queries[:, tile * 128 : tile * 128 + 128].T
@@ -141,26 +145,36 @@
         message[head, 64:96, :] = turn(block[64:96])
         message[head, 96:128, :] = rope_t
     loads[0].wait()
+    loads[12].wait()
     normed = rms_scaled(latent[...], latent_gain_ref[...]).astype(jnp.bfloat16)
     loads[1].wait()
     keys_values = jnp.dot(normed, latent_up[...], preferred_element_type=jnp.float32).astype(
         jnp.bfloat16
     )
     for head in range(16):
-        message[head, 128:256, :] = keys_values[:, head * 128 : head * 128 + 128]
+        message[head, 128:256, :] = keys_values[:, head * 128 : head * 128 + 128].T
     pl.semaphore_wait(barrier, 127)
 
-    def deliver(k, carry):
-        peer = peer_at(here, k)
-        pltpu.make_async_remote_copy(
-            message.at[peer], letters.at[sp], msg_sem, letter_sem,
-            device_id=(peer, dp), device_id_type=MESH,
-        ).start()
-        return carry
-
-    lax.fori_loop(1, 16, deliver, 0)
+    def deliver(rows, sem):
+        def one(k, carry):
+            peer = peer_at(here, k)
+            pltpu.make_async_remote_copy(
+                message.at[peer, rows], letters.at[sp, rows], msg_sem, sem,
+                device_id=(peer, dp), device_id_type=MESH,
+            ).start()
+            return carry
+
+        lax.fori_loop(1, 16, one, 0)
+
+    keys_part, values_part = pl.ds(0, 192), pl.ds(192, 64)
+    deliver(keys_part, letter_sem)
+    deliver(values_part, value_sem)
     letters[sp] = message[sp]
-
+    for i in (14, 15, 4, 5, 16, 17, 18, 6, 7, 8, 9, 10, 11, 19, 20):
+        loads[i].start()
+
+    loads[14].wait()
+    loads[15].wait()
     ids_t = ids_t_ref[...]
     named_t = jnp.zeros((128, 128), jnp.bool_)
     for col in range(TOP_K):
@@ -174,37 +188,32 @@
             axis=0, keepdims=True,
         )
         places_t[col : col + 1, :] = order_t[col : col + 1, :] * SLOTS + slot.astype(jnp.int32)
-    ids = ids_ref[...]
-    named = jnp.zeros((128, 128), jnp.bool_)
-    for col in range(TOP_K):
-        named = named | (iota((128, 128), 1) == ids[:, col : col + 1])
-    after = (iota((128, 128), 1) < iota((128, 128), 0)).astype(jnp.bfloat16)
-    count = jnp.dot(after, named.astype(jnp.bfloat16), preferred_element_type=jnp.float32)
-    order = order_of(ids, here)
-    for col in range(TOP_K):
-        slot = jnp.sum(
-            jnp.where(iota((128, 128), 1) == ids[:, col : col + 1], count, 0.0),
-            axis=1, keepdims=True,
-        )
-        places[:, col : col + 1] = order[:, col : col + 1] * SLOTS + slot.astype(jnp.int32)
-    weights = weights_ref[...]
-    gates[...] = weights / jnp.sum(weights, axis=-1, keepdims=True) * ROUTED
+    def upright(short):
+        filler = jnp.zeros((128 - TOP_K, 128), short.dtype)
+        return jnp.concatenate([short, filler], axis=0).T[:, 0:TOP_K]
+
+    places[...] = upright(places_t[...].astype(jnp.float32)).astype(jnp.int32)
+    weights = weights_t_ref[...]
+    gates[...] = upright(weights / jnp.sum(weights, axis=0, keepdims=True) * ROUTED)
 
     asked[...] = jnp.zeros_like(asked)
     fifteen = message.at[pl.ds(0, 15)]
-    pltpu.make_async_copy(fifteen, fifteen, letter_sem).wait()
+    some = message.at[pl.ds(0, 15), keys_part]
+    pltpu.make_async_copy(some, some, letter_sem).wait()
     for block in range(16):
         span = slice(block * 128, block * 128 + 128)
-        top, pair = letters[block, 0:128, :], letters[block, 128:256, :]
-        keys[span, 0:128] = pair
-        keys[span, 128:256] = top.T
-        asked[0:64, span] = top[0:64]
-        asked[224:256, span] = top[64:96]
-        values_t[:, span] = pair.T
+        top, plain = letters[block, 0:128, :], letters[block, 128:192, :]
+        keys[span, 0:128] = top.T
+        keys[span, 128:192] = plain.T
+        asked[96:128, span] = top[64:96]
+        asked[128:192, span] = top[0:64]
 
     factor = math.log2(math.e) / math.sqrt(PLAIN_HEAD_WIDTH + QK_ROPE)
 
-    def attend(index):
+    def place_of(index, other):
+        return index * (index + 1) // 2 + other
+
+    def score(index):
         asking = asked[:, index * 256 : index * 256 + 256]
         peak = None
         for other in range(index + 1):
@@ -212,26 +221,27 @@
             part = jnp.dot(keys[span, :], asking, preferred_element_type=jnp.float32)
             if other == index:
                 part = jnp.where(iota((256, 256), 0) <= iota((256, 256), 1), part, -jnp.inf)
-            scores[span, :] = part
+            scores[place_of(index, other)] = part
             high = jnp.max(part, axis=0, keepdims=True)
             peak = high if peak is None else jnp.maximum(peak, high)
-        peak = peak * factor
+        return peak * factor
+
+    def attend(index, peak):
         weight, mixed = 0.0, 0.0
         for other in range(index + 1):
-            span = slice(other * 256, other * 256 + 256)
-            part = jnp.exp2(scores[span, :] * factor - peak)
+            part = jnp.exp2(scores[place_of(index, other)] * factor - peak)
             weight = weight + jnp.sum(part, axis=0, keepdims=True)
             mixed = mixed + jnp.dot(
-                values_t[64:128, span], part.astype(jnp.bfloat16),
+                values_t[:, other * 256 : other * 256 + 256], part.astype(jnp.bfloat16),
                 preferred_element_type=jnp.float32,
             )
         mixed = (mixed / weight).astype(jnp.bfloat16)
         heads_out[2 * index] = mixed[:, 0:128]
         heads_out[2 * index + 1] = mixed[:, 128:256]
 
-    def give_back(base):
+    def give_back(base, count):
         def give(k, carry):
-            peer = base + (sp + k) % 8
+            peer = base + (sp + k) % count
 
             @pl.when(peer != sp)
             def _():
@@ -242,17 +252,20 @@
 
             return carry
 
-        lax.fori_loop(0, 8, give, 0)
-
-    for index in (7, 6, 5, 4):
-        attend(index)
-    give_back(8)
-    for index in (3, 2, 1, 0):
-        attend(index)
-    give_back(0)
+        lax.fori_loop(0, count, give, 0)
+
+    peaks = [score(index) for index in range(8)]
+    some = message.at[pl.ds(0, 15), values_part]
+    pltpu.make_async_copy(some, some, value_sem).wait()
+    for block in range(16):
+        values_t[:, block * 128 : block * 128 + 128] = letters[block, 192:256, :]
+    for index in range(8):
+        attend(index, peaks[index])
+        if index in (3, 5, 7):
+            give_back(*{3: (0, 8), 5: (8, 4), 7: (12, 4)}[index])
     heads_in[sp] = heads_out[sp]
-    loads[4].wait()
-    loads[5].wait()
+    for load in loads[4:6] + loads[16:21]:
+        load.wait()
     arrivals = heads_out.at[pl.ds(0, 15)]
     pltpu.make_async_copy(arrivals, arrivals, heads_sem).wait()
     attended = heads_in[...].reshape(1024, 128).T
@@ -330,7 +343,7 @@
     total[...] = ALPHA * tokens.astype(jnp.float32) + jnp.dot(
         inner, sdown[...], preferred_element_type=jnp.float32
     )
-    for load in loads[9:]:
+    for load in loads[9:12]:
         load.wait()
 
     def expert_group(group, carry):
@@ -381,16 +394,24 @@
 ):
     bf16, f32 = jnp.bfloat16, jnp.float32
     vmem = pl.BlockSpec(memory_space=pltpu.VMEM)
-    hbm = pl.BlockSpec(memory_space=pl.ANY)
+    hbm = pl.BlockSpec(memory_space=pltpu.HBM)
     blocks = pltpu.VMEM((GROUPS * PER_GROUP, SLOTS * TILES, 128), bf16)
     tables = jnp.asarray(rotation_tables(16, 128))
-    ids = expert_ids[0]
-    result = pl.pallas_call(
+    layer = pl.pallas_call(
         layer_kernel,
         out_shape=jax.ShapeDtypeStruct((128, D), bf16),
-        in_specs=[vmem] * 10 + [hbm] * 12,
+        in_specs=[hbm] * 21,
         out_specs=vmem,
         scratch_shapes=[
+            pltpu.VMEM((TOP_K, 128), jnp.int32),
+            pltpu.VMEM((TOP_K, 128), f32),
+            pltpu.VMEM((QK_ROPE, 128), bf16),
+            pltpu.VMEM((1, 512), f32),
+            pltpu.VMEM((1, 1024), f32),
+            pltpu.VMEM((1, D), f32),
+            pltpu.VMEM((1, D), f32),
+            pltpu.VMEM((1, D), f32),
+            pltpu.VMEM((1, D), f32),
             pltpu.VMEM((128, 512), bf16),
             pltpu.VMEM((512, 2048), bf16),
             pltpu.VMEM((128, 1536), bf16),
@@ -406,10 +427,10 @@
             pltpu.VMEM((1536, 128), bf16),
             pltpu.VMEM((16, 256, 128), bf16),
             pltpu.VMEM((16, 256, 128), bf16),
-            pltpu.VMEM((2048, 256), bf16),
-            pltpu.VMEM((256, 2048), bf16),
-            pltpu.VMEM((128, 2048), bf16),
-            pltpu.VMEM((2048, 256), f32),
+            pltpu.VMEM((2048, 192), bf16),
+            pltpu.VMEM((192, 2048), bf16),
+            pltpu.VMEM((64, 2048), bf16),
+            pltpu.VMEM((36, 256, 256), f32),
             pltpu.VMEM((16, 64, 128), bf16),
             pltpu.VMEM((16, 64, 128), bf16),
             pltpu.VMEM((128, D), bf16),
@@ -420,7 +441,8 @@
             pltpu.VMEM((GROUP_ROWS * TILES, 128), f32),
             pltpu.VMEM((GROUP_ROWS, D), bf16),
             pltpu.VMEM((128, D), f32),
-            pltpu.SemaphoreType.DMA((12,)),
+            pltpu.SemaphoreType.DMA((21,)),
+            pltpu.SemaphoreType.DMA,
             pltpu.SemaphoreType.DMA,
             pltpu.SemaphoreType.DMA,
             pltpu.SemaphoreType.DMA,
@@ -431,14 +453,16 @@
             pltpu.SemaphoreType.DMA((GROUPS,)),
         ],
         compiler_params=pltpu.CompilerParams(
-            collective_id=1, has_side_effects=True, vmem_limit_bytes=58 * 2**20
+            collective_id=1, has_side_effects=True, vmem_limit_bytes=52 * 2**20
         ),
-    )(
-        ids, ids.T, route_weights[0], keys_rope[0], latent_norm_gain[None], attn_gain[None],
-        norm1_gain[None], norm1_bias[None], norm2_gain[None], norm2_bias[None],
+    )
+    operands = (
+        expert_ids[0].T, route_weights[0].T, keys_rope[0].T, latent_norm_gain[None],
+        attn_gain[None], norm1_gain[None], norm1_bias[None], norm2_gain[None], norm2_bias[None],
         key_value_latent[0], latent_up_weight, queries[0], tables, hidden_in[0],
         out_proj, gate_proj, up_proj, down_proj, shared_gate, shared_up, shared_down,
     )
+    result = layer(*(pltpu.with_memory_space_constraint(a, pltpu.HBM) for a in operands))
     return result[None]
 
 

time: 125 us -> 112 us (0.90); the launches traced: 123 us -> 112 us
  Pallas kernels: 117 us -> 111 us
  local copies, waits for them, and re-layouts: 6.1 us -> 0.8 us
    pallas_call x1, Pallas kernels: 117 us -> 111 us  [per_device(): layer(*(pltpu.with_memory_space_constraint(a, pltpu.HBM) for a in operands))]
    unnamed x3 -> x1, local copies, waits for them, and re-layouts: 4.69 us -> 0.8 us
    squeeze x1 -> x0, local copies, waits for them, and re-layouts: 1.42 us -> none  [per_device(): ids = expert_ids[0]]
where the time goes in v3:
time: 112 us
  Pallas kernels  111 us (99%)
    pallas_call x1, Pallas kernels, per_device(): layer(*(pltpu.with_memory_space_constraint(a, pltpu.HBM) for a in operands))  111 us

profile of v3, /device:TPU:1, one launch (start us, length us, event | category | flops | bytes accessed | tf_op | source)
XLA Modules:
  0.0 112.1 jit_solution(14755552542174696311)
XLA Ops:
  0.0 111.3 %shard_map.199 = bf16[128,2048]{1,0:T(8,128)(2,1)S(1)} custom-call(s32[4,128]{1,0:T(4,128)} %bitcast.29, f32[4,128]{1,0:T(4,128)} %bitcast.30, bf16[32,128]{1,0:T(8,128)(2,1)} %bitcast.23, f32[1,512]{1,0:T(1,128)} %bitcast.31, f32[1,1024]{1,0:T(1,128)} %bitcast.28, f32[1,2048]{1,0:T(1,128)} %bitcast.24, f32[1,2048]{1,0:T(1,128)} %bitcast.25, ...), custom_call_target="tpu_custom_call" | custom-call | tf_op jit(solution)/shard_map/pallas_call | solution.py:465
  111.3 0.8 copy.23

commit v4 on v3

--- a/solution.py
+++ b/solution.py
@@ -51,25 +51,6 @@
 
 def position_of(sp, dp):
     return sp // 4, sp % 4, dp // 2, dp % 2
-
-
-def step_of(k):
-    dc, dy, dx = (k // 16) % 2, (k // 4) % 4, k % 4
-    return (k // 32 + 8 - dx - dy) % 4, dy, dx, dc
-
-
-def peer_at(here, k):
-    z, y = here[:2]
-    dy = k % 4
-    return (z + (k // 4 + 4 - dy)) % 4 * 4 + (y + dy) % 4
-
-
-def device_at(here, k, sign):
-    z, y, x, c = here
-    dz, dy, dx, dc = step_of(k)
-    z, y = (z + 4 + sign * dz) % 4, (y + 4 + sign * dy) % 4
-    x, c = (x + 4 + sign * dx) % 4, (c + dc) % 2
-    return (z * 4 + y, x * 2 + c)
 
 
 def order_of(expert_ids, here):
@@ -93,7 +74,7 @@
     gain1_ref, bias1_ref, gain2_ref, bias2_ref,
     latent, latent_up, queries, tables, hidden,
     out_proj, gate, up, down, sgate, sup, sdown,
-    turned, message, letters, keys, asked, values_t, scores, heads_out, heads_in,
+    turned, message, letters, keys, asked, values_t, scores, probs, heads_out, heads_in,
     first, places_t, places, gates, send, arrived, made, returned, flat, rows, total,
     load_sem, msg_sem, letter_sem, value_sem, head_sem, heads_sem,
     send_sem, recv_sem, back_sem, ret_sem,
@@ -119,11 +100,27 @@
         loads[i].start()
     barrier = pltpu.get_barrier_semaphore()
 
-    def greet(k, carry):
-        pl.semaphore_signal(barrier, inc=1, device_id=device_at(here, k, 1), device_id_type=MESH)
+    columns = [lax.rem(dp + j, 8) for j in range(8)]
+
+    def greet(i, carry):
+        row = lax.rem(sp + i, 16)
+
+        def signal(column):
+            pl.semaphore_signal(barrier, inc=1, device_id=(row, column), device_id_type=MESH)
+
+        for j in range(1, 8):
+            signal(columns[j])
+
+        @pl.when(i > 0)
+        def _():
+            signal(columns[0])
+
         return carry
 
-    lax.fori_loop(1, 128, greet, 0)
+    lax.fori_loop(0, 16, greet, 0)
+    z, y, x, c = here
+    z_plus, y_plus, x_plus = ([lax.rem(v + j, 4) for j in range(4)] for v in (z, y, x))
+    y_minus, x_minus = ([lax.rem(v + 4 - j, 4) for j in range(4)] for v in (y, x))
 
     loads[3].wait()
     loads[13].wait()
@@ -156,15 +153,12 @@
     pl.semaphore_wait(barrier, 127)
 
     def deliver(rows, sem):
-        def one(k, carry):
-            peer = peer_at(here, k)
+        for k in range(1, 16):
+            peer = z_plus[(k // 4 - k) % 4] * 4 + y_plus[k % 4]
             pltpu.make_async_remote_copy(
                 message.at[peer, rows], letters.at[sp, rows], msg_sem, sem,
                 device_id=(peer, dp), device_id_type=MESH,
             ).start()
-            return carry
-
-        lax.fori_loop(1, 16, one, 0)
 
     keys_part, values_part = pl.ds(0, 192), pl.ds(192, 64)
     deliver(keys_part, letter_sem)
@@ -213,26 +207,31 @@
     def place_of(index, other):
         return index * (index + 1) // 2 + other
 
-    def score(index):
+    def weigh(index):
         asking = asked[:, index * 256 : index * 256 + 256]
-        peak = None
+        peak, weight = None, 0.0
         for other in range(index + 1):
-            span = slice(other * 256, other * 256 + 256)
-            part = jnp.dot(keys[span, :], asking, preferred_element_type=jnp.float32)
+            part = jnp.dot(
+                keys[other * 256 : other * 256 + 256, :], asking,
+                preferred_element_type=jnp.float32,
+            )
             if other == index:
                 part = jnp.where(iota((256, 256), 0) <= iota((256, 256), 1), part, -jnp.inf)
-            scores[place_of(index, other)] = part
+            scores[index % 2, other] = part
             high = jnp.max(part, axis=0, keepdims=True)
             peak = high if peak is None else jnp.maximum(peak, high)
-        return peak * factor
-
-    def attend(index, peak):
-        weight, mixed = 0.0, 0.0
+        peak = peak * factor
         for other in range(index + 1):
-            part = jnp.exp2(scores[place_of(index, other)] * factor - peak)
+            part = jnp.exp2(scores[index % 2, other] * factor - peak)
             weight = weight + jnp.sum(part, axis=0, keepdims=True)
+            probs[place_of(index, other)] = part.astype(jnp.bfloat16)
+        return weight
+
+    def attend(index, weight):
+        mixed = 0.0
+        for other in range(index + 1):
             mixed = mixed + jnp.dot(
-                values_t[:, other * 256 : other * 256 + 256], part.astype(jnp.bfloat16),
+                values_t[:, other * 256 : other * 256 + 256], probs[place_of(index, other)],
                 preferred_element_type=jnp.float32,
             )
         mixed = (mixed / weight).astype(jnp.bfloat16)
@@ -254,13 +253,13 @@
 
         lax.fori_loop(0, count, give, 0)
 
-    peaks = [score(index) for index in range(8)]
+    sums = [weigh(index) for index in range(8)]
     some = message.at[pl.ds(0, 15), values_part]
     pltpu.make_async_copy(some, some, value_sem).wait()
     for block in range(16):
         values_t[:, block * 128 : block * 128 + 128] = letters[block, 192:256, :]
     for index in range(8):
-        attend(index, peaks[index])
+        attend(index, sums[index])
         if index in (3, 5, 7):
             give_back(*{3: (0, 8), 5: (8, 4), 7: (12, 4)}[index])
     heads_in[sp] = heads_out[sp]
@@ -293,19 +292,25 @@
                 pl.ds(tile, GROUP_ROWS, stride=TILES), :
             ].astype(jnp.bfloat16)
 
-    def dispatch(k, carry):
-        pltpu.make_async_remote_copy(
-            send.at[k], arrived.at[k], send_sem, recv_sem.at[k // PER_GROUP],
-            device_id=device_at(here, k, 1), device_id_type=MESH,
-        ).start()
-        return carry
-
-    def reply(k, carry):
-        pltpu.make_async_remote_copy(
-            made.at[k], returned.at[k], back_sem, ret_sem.at[k // PER_GROUP],
-            device_id=device_at(here, k, -1), device_id_type=MESH,
-        ).start()
-        return carry
+    def post(group, source, target, out_sem, in_sem, sign):
+        turn_z, core = z + 8 + sign * (group // 2), lax.rem(c + group % 2, 2)
+        z_of = [lax.rem(turn_z - sign * j, 4) for j in range(4)]
+        y_of, x_of = (y_plus, x_plus) if sign > 0 else (y_minus, x_minus)
+        for i in range(PER_GROUP):
+            dy, dx = i // 4, i % 4
+
+            def start(i=i, dy=dy, dx=dx):
+                k = group * PER_GROUP + i
+                peer = (z_of[(dy + dx) % 4] * 4 + y_of[dy], x_of[dx] * 2 + core)
+                pltpu.make_async_remote_copy(
+                    source.at[k], target.at[k], out_sem, in_sem.at[group],
+                    device_id=peer, device_id_type=MESH,
+                ).start()
+
+            if i == 0:
+                pl.when(group > 0)(start)
+            else:
+                start()
 
     def wait_blocks(group, buffer, sem):
         @pl.when(group == 0)
@@ -328,7 +333,7 @@
         )
         pack(group, out, send)
 
-        lax.fori_loop(jnp.maximum(group * PER_GROUP, 1), (group + 1) * PER_GROUP, dispatch, 0)
+        post(group, send, arrived, send_sem, recv_sem, 1)
         return carry
 
     lax.fori_loop(0, GROUPS, load_group, 0)
@@ -355,7 +360,7 @@
         inner = (gated / (1.0 + jnp.exp(-gated)) * lifted).astype(jnp.bfloat16)
         out = jnp.dot(inner, down[...], preferred_element_type=jnp.float32)
         pack(group, out, made)
-        lax.fori_loop(jnp.maximum(group * PER_GROUP, 1), (group + 1) * PER_GROUP, reply, 0)
+        post(group, made, returned, back_sem, ret_sem, -1)
         return carry
 
     lax.fori_loop(0, GROUPS, expert_group, 0)
@@ -430,7 +435,8 @@
             pltpu.VMEM((2048, 192), bf16),
             pltpu.VMEM((192, 2048), bf16),
             pltpu.VMEM((64, 2048), bf16),
-            pltpu.VMEM((36, 256, 256), f32),
+            pltpu.VMEM((2, 8, 256, 256), f32),
+            pltpu.VMEM((36, 256, 256), bf16),
             pltpu.VMEM((16, 64, 128), bf16),
             pltpu.VMEM((16, 64, 128), bf16),
             pltpu.VMEM((128, D), bf16),

time: 112 us -> 106 us (0.946)
  Pallas kernels: 111 us -> 105 us
    pallas_call x1, Pallas kernels: 111 us -> 105 us  [per_device(): layer(*(pltpu.with_memory_space_constraint(a, pltpu.HBM) for a in operands))]
where the time goes in v4:
time: 106 us
  Pallas kernels  105 us (99%)
    pallas_call x1, Pallas kernels, per_device(): layer(*(pltpu.with_memory_space_constraint(a, pltpu.HBM) for a in operands))  105 us

profile of v4, /device:TPU:1, one launch (start us, length us, event | category | flops | bytes accessed | tf_op | source)
XLA Modules:
  0.0 105.9 jit_solution(18007180101197221710)
XLA Ops:
  0.0 105.1 %shard_map.199 = bf16[128,2048]{1,0:T(8,128)(2,1)S(1)} custom-call(s32[4,128]{1,0:T(4,128)} %bitcast.29, f32[4,128]{1,0:T(4,128)} %bitcast.30, bf16[32,128]{1,0:T(8,128)(2,1)} %bitcast.23, f32[1,512]{1,0:T(1,128)} %bitcast.31, f32[1,1024]{1,0:T(1,128)} %bitcast.28, f32[1,2048]{1,0:T(1,128)} %bitcast.24, f32[1,2048]{1,0:T(1,128)} %bitcast.25, ...), custom_call_target="tpu_custom_call" | custom-call | tf_op jit(solution)/shard_map/pallas_call | solution.py:471
  105.1 0.8 copy.23

commit v5 on v4

--- a/solution.py
+++ b/solution.py
@@ -296,7 +296,7 @@
         turn_z, core = z + 8 + sign * (group // 2), lax.rem(c + group % 2, 2)
         z_of = [lax.rem(turn_z - sign * j, 4) for j in range(4)]
         y_of, x_of = (y_plus, x_plus) if sign > 0 else (y_minus, x_minus)
-        for i in range(PER_GROUP):
+        for i in (0, 5, 10, 15, 1, 6, 11, 12, 2, 7, 8, 13, 3, 4, 9, 14):
             dy, dx = i // 4, i % 4
 
             def start(i=i, dy=dy, dx=dx):

time: 106 us -> 105 us (level)
  no operation moved by 1% of the time
where the time goes in v5:
time: 105 us
  Pallas kernels  104 us (99%)
    pallas_call x1, Pallas kernels, per_device(): layer(*(pltpu.with_memory_space_constraint(a, pltpu.HBM) for a in operands))  104 us

profile of v5, /device:TPU:1, one launch (start us, length us, event | category | flops | bytes accessed | tf_op | source)
XLA Modules:
  0.0 105.0 jit_solution(3596073460042782103)
XLA Ops:
  0.0 104.2 %shard_map.199 = bf16[128,2048]{1,0:T(8,128)(2,1)S(1)} custom-call(s32[4,128]{1,0:T(4,128)} %bitcast.29, f32[4,128]{1,0:T(4,128)} %bitcast.30, bf16[32,128]{1,0:T(8,128)(2,1)} %bitcast.23, f32[1,512]{1,0:T(1,128)} %bitcast.31, f32[1,1024]{1,0:T(1,128)} %bitcast.28, f32[1,2048]{1,0:T(1,128)} %bitcast.24, f32[1,2048]{1,0:T(1,128)} %bitcast.25, ...), custom_call_target="tpu_custom_call" | custom-call | tf_op jit(solution)/shard_map/pallas_call | solution.py:471
  104.2 0.8 copy.23

commit v6 on v5

--- a/solution.py
+++ b/solution.py
@@ -77,7 +77,7 @@
     turned, message, letters, keys, asked, values_t, scores, probs, heads_out, heads_in,
     first, places_t, places, gates, send, arrived, made, returned, flat, rows, total,
     load_sem, msg_sem, letter_sem, value_sem, head_sem, heads_sem,
-    send_sem, recv_sem, back_sem, ret_sem,
+    send_sem, recv_sem, back_sem, ret_sem, all_sem,
 ):
     sp, dp = lax.axis_index("sp"), lax.axis_index("dp")
     here = position_of(sp, dp)
@@ -103,21 +103,13 @@
     columns = [lax.rem(dp + j, 8) for j in range(8)]
 
     def greet(i, carry):
-        row = lax.rem(sp + i, 16)
-
-        def signal(column):
-            pl.semaphore_signal(barrier, inc=1, device_id=(row, column), device_id_type=MESH)
-
-        for j in range(1, 8):
-            signal(columns[j])
-
-        @pl.when(i > 0)
-        def _():
-            signal(columns[0])
-
+        peer = (lax.rem(sp + i, 16), dp)
+        pl.semaphore_signal(barrier, inc=1, device_id=peer, device_id_type=MESH)
         return carry
 
-    lax.fori_loop(0, 16, greet, 0)
+    lax.fori_loop(1, 16, greet, 0)
+    for j in range(1, 8):
+        pl.semaphore_signal(barrier, inc=1, device_id=(sp, columns[j]), device_id_type=MESH)
     z, y, x, c = here
     z_plus, y_plus, x_plus = ([lax.rem(v + j, 4) for j in range(4)] for v in (z, y, x))
     y_minus, x_minus = ([lax.rem(v + 4 - j, 4) for j in range(4)] for v in (y, x))
@@ -150,7 +142,7 @@
     )
     for head in range(16):
         message[head, 128:256, :] = keys_values[:, head * 128 : head * 128 + 128].T
-    pl.semaphore_wait(barrier, 127)
+    pl.semaphore_wait(barrier, 22)
 
     def deliver(rows, sem):
         for k in range(1, 16):
@@ -163,6 +155,8 @@
     keys_part, values_part = pl.ds(0, 192), pl.ds(192, 64)
     deliver(keys_part, letter_sem)
     deliver(values_part, value_sem)
+    for j in range(1, 8):
+        pl.semaphore_signal(all_sem, inc=1, device_id=(sp, columns[j]), device_id_type=MESH)
     letters[sp] = message[sp]
     for i in (14, 15, 4, 5, 16, 17, 18, 6, 7, 8, 9, 10, 11, 19, 20):
         loads[i].start()
@@ -322,6 +316,8 @@
         def _():
             block = buffer.at[pl.ds(0, PER_GROUP)]
             pltpu.make_async_copy(block, block, sem.at[group]).wait()
+
+    pl.semaphore_wait(all_sem, 7)
 
     def load_group(group, carry):
         picks = iota((GROUP_ROWS, 128), 0) + group * GROUP_ROWS
@@ -457,6 +453,7 @@
             pltpu.SemaphoreType.DMA((GROUPS,)),
             pltpu.SemaphoreType.DMA,
             pltpu.SemaphoreType.DMA((GROUPS,)),
+            pltpu.SemaphoreType.REGULAR,
         ],
         compiler_params=pltpu.CompilerParams(
             collective_id=1, has_side_effects=True, vmem_limit_bytes=52 * 2**20

time: 105 us -> 104 us (level)
    pallas_call x1, Pallas kernels: 104 us -> 103 us  [per_device(): layer(*(pltpu.with_memory_space_constraint(a, pltpu.HBM) for a in operands))]
where the time goes in v6:
time: 104 us
  Pallas kernels  103 us (99%)
    pallas_call x1, Pallas kernels, per_device(): layer(*(pltpu.with_memory_space_constraint(a, pltpu.HBM) for a in operands))  103 us

profile of v6, /device:TPU:1, one launch (start us, length us, event | category | flops | bytes accessed | tf_op | source)
XLA Modules:
  0.0 103.7 jit_solution(13570818069592698254)
XLA Ops:
  0.0 102.9 %shard_map.199 = bf16[128,2048]{1,0:T(8,128)(2,1)S(1)} custom-call(s32[4,128]{1,0:T(4,128)} %bitcast.29, f32[4,128]{1,0:T(4,128)} %bitcast.30, bf16[32,128]{1,0:T(8,128)(2,1)} %bitcast.23, f32[1,512]{1,0:T(1,128)} %bitcast.31, f32[1,1024]{1,0:T(1,128)} %bitcast.28, f32[1,2048]{1,0:T(1,128)} %bitcast.24, f32[1,2048]{1,0:T(1,128)} %bitcast.25, ...), custom_call_target="tpu_custom_call" | custom-call | tf_op jit(solution)/shard_map/pallas_call | solution.py:468
  102.9 0.8 copy.23
